TPU v7x, 512 devices: a whole 4x8x8 slice. The times are simulated.
512 devices in a mesh: ep: 128 (over z, y, core), tp: 4 (over x).
Axes of the slice: x: 4, y: 8, z: 8, core: 2. Of those that a mesh axis runs over, the one named last changes fastest.
Arguments:
- tokens: bfloat16 [16384, 2048], P('ep'), may hold values from -6 to 6
- expert_ids: int32 [16384, 2], P('ep'), may hold values from 0 to 127, as said below
- route_weights: bfloat16 [16384, 2], P('ep'), may hold values from 0.099609375 to 1
- cotangent: bfloat16 [16384, 2048], P('ep'), may hold values from -3 to 3
- w_gate: bfloat16 [128, 2048, 512], P('ep', None, 'tp'), may hold values from -0.125 to 0.125
- w_up: bfloat16 [128, 2048, 512], P('ep', None, 'tp'), may hold values from -0.125 to 0.125
- w_down: bfloat16 [128, 512, 2048], P('ep', 'tp'), may hold values from -0.25 to 0.25
Outputs:
- token_grad: bfloat16 [16384, 2048], P('ep', 'tp')
- route_grad: bfloat16 [16384, 2], P('ep')
- grad_gate: bfloat16 [128, 2048, 512], P('ep', None, 'tp')
- grad_up: bfloat16 [128, 2048, 512], P('ep', None, 'tp')
- grad_down: bfloat16 [128, 512, 2048], P('ep', 'tp')
- gate_rows: float32 [128, 2048], P('ep')
- up_rows: float32 [128, 2048], P('ep')
- down_rows: float32 [128, 512], P('ep', 'tp')
Inputs may be any that keep to these rules, and one draw needn't show every extreme that they name: `expert_ids`: each row names 2 different experts of one group: both lie in g * 32 to (g + 1) * 32 - 1 for the row's group g. In the rows of one device (aligned blocks of 128 rows) no expert is named more than 4 times, and in every block some expert is named exactly 4 times.
All inputs are finite; a program needn't handle non-finite values.
Results may differ from a plain program's by a relative error of at most 0.012.
Values may be sent and summed in bfloat16 or wider, within the bound.
A program may use at most 64 MiB of HBM per device.

v0:
```python
import jax
import jax.numpy as jnp
from jax import lax
from jax.sharding import PartitionSpec as P

TOPK = 2


def side_by_side(arrays, axis, split_dim, concat_dim, along):
    columns = [a.reshape(*a.shape[:along], -1) for a in arrays]
    both = jnp.concatenate(columns, axis=along)
    result, at, done = (
        lax.all_to_all(both, axis, split_axis=split_dim, concat_axis=concat_dim, tiled=True),
        0,
        [],
    )
    for a, column in zip(arrays, columns):
        section = result[..., at : at + column.shape[along]]
        done.append(section.reshape(*section.shape[:along], *a.shape[along:]))
        at += column.shape[along]
    return tuple(done)


def in_one_piece(arrays, axis, dim, along):
    both = jnp.concatenate(arrays, axis=along)
    result, at, done = (lax.all_gather(both, axis, axis=dim, tiled=True), 0, [])
    for a in arrays:
        done.append(lax.slice_in_dim(result, at, at + a.shape[along], axis=along))
        at += a.shape[along]
    return tuple(done)


def from_everyone(shard, axis):
    count = lax.axis_size(axis)
    return lax.all_to_all(
        jnp.broadcast_to(shard[None], (count, *shard.shape)), axis, 0, 0, tiled=True
    )


def over_copies(shard, axis):
    return from_everyone(shard, axis).sum(axis=0)


def together(arrays, axis):
    line, at, done = (jnp.concatenate([a.reshape(-1) for a in arrays]), 0, [])
    subtotal = over_copies(line, axis)
    for a in arrays:
        done.append(subtotal[at : at + a.size].reshape(a.shape))
        at += a.size
    return tuple(done)


def on_device(tokens, expert_ids, route_weights, cotangent, w_gate, w_up, w_down):
    tok_rows, model_width = tokens.shape
    experts = lax.axis_size("ep")
    splits = lax.axis_size("tp")
    capacity = 2 * tok_rows * TOPK // experts
    slot_count = experts * capacity
    assigns = tok_rows * TOPK
    flat_ids = expert_ids.reshape(-1)
    onehot = (flat_ids[:, None] == jnp.arange(experts, dtype=jnp.int32)[None, :]).astype(
        jnp.float32
    )
    assign_order = jnp.arange(assigns, dtype=jnp.int32)
    earlier = (assign_order[:, None] > assign_order[None, :]).astype(jnp.float32)
    before = jnp.dot(earlier, onehot, precision=lax.Precision.HIGHEST)
    slot_rank = jnp.sum(before * onehot, axis=1).astype(jnp.int32)
    position = flat_ids * capacity + slot_rank
    slot_owner = jnp.full((slot_count,), tok_rows, jnp.int32).at[position].set(assign_order // TOPK)
    slot_scale = jnp.zeros((slot_count,), jnp.bfloat16).at[position].set(route_weights.reshape(-1))
    slice_width = model_width // splits
    slice_start = lax.axis_index("tp") * slice_width
    rows_slice = lax.dynamic_slice_in_dim(tokens, slice_start, slice_width, 1)
    cot_slice = lax.dynamic_slice_in_dim(cotangent, slice_start, slice_width, 1)
    rows_pad = jnp.concatenate([rows_slice, jnp.zeros((1, slice_width), jnp.bfloat16)], axis=0)
    cot_pad = jnp.concatenate([cot_slice, jnp.zeros((1, slice_width), jnp.bfloat16)], axis=0)
    outgoing = rows_pad[slot_owner]
    outgoing_cot = cot_pad[slot_owner]
    part_rows, part_cot, got_scale = side_by_side(
        (outgoing, outgoing_cot, slot_scale), "ep", 0, 0, 1
    )
    slot_rows, slot_cot = in_one_piece((part_rows, part_cot), "tp", 1, 0)
    scale_col = got_scale.reshape(slot_count, 1).astype(jnp.float32)
    gate_cols = w_gate[0]
    up_cols = w_up[0]
    down_part = w_down[0]
    gate_pre = jnp.dot(slot_rows, gate_cols, preferred_element_type=jnp.float32)
    up_pre = jnp.dot(slot_rows, up_cols, preferred_element_type=jnp.float32)
    hidden_back = lax.dot_general(
        slot_cot, down_part, (((1,), (1,)), ((), ())), preferred_element_type=jnp.float32
    )
    gate_sig = jax.nn.sigmoid(gate_pre)
    activated = gate_pre * gate_sig
    hidden = activated * up_pre
    route_part = jnp.sum(hidden * hidden_back, axis=1)
    hidden_cot = scale_col * hidden_back
    up_cot = (hidden_cot * activated).astype(jnp.bfloat16)
    gate_cot = (hidden_cot * up_pre * gate_sig * (1.0 + gate_pre * (1.0 - gate_sig))).astype(
        jnp.bfloat16
    )
    weighted_hidden = (scale_col * hidden).astype(jnp.bfloat16)
    grad_down = lax.dot_general(
        weighted_hidden, slot_cot, (((0,), (0,)), ((), ())), preferred_element_type=jnp.float32
    ).astype(jnp.bfloat16)
    grad_gate = lax.dot_general(
        slot_rows, gate_cot, (((0,), (0,)), ((), ())), preferred_element_type=jnp.float32
    ).astype(jnp.bfloat16)
    grad_up = lax.dot_general(
        slot_rows, up_cot, (((0,), (0,)), ((), ())), preferred_element_type=jnp.float32
    ).astype(jnp.bfloat16)
    token_term = lax.dot_general(
        gate_cot, gate_cols, (((1,), (1,)), ((), ())), preferred_element_type=jnp.float32
    )
    token_term = token_term + lax.dot_general(
        up_cot, up_cols, (((1,), (1,)), ((), ())), preferred_element_type=jnp.float32
    )
    reduced = lax.psum_scatter(
        token_term.astype(jnp.bfloat16), "tp", scatter_dimension=1, tiled=True
    )
    gate_square = jnp.sum(jnp.square(grad_gate.astype(jnp.float32)), axis=1)
    up_square = jnp.sum(jnp.square(grad_up.astype(jnp.float32)), axis=1)
    down_square = jnp.sum(jnp.square(grad_down.astype(jnp.float32)), axis=1)
    route_total, gate_rows, up_rows = together((route_part, gate_square, up_square), "tp")
    back_rows, back_route = side_by_side((reduced, route_total.astype(jnp.bfloat16)), "ep", 0, 0, 1)
    per_assign = back_rows[position].astype(jnp.float32).reshape(tok_rows, TOPK, -1)
    token_grad = jnp.sum(per_assign, axis=1).astype(jnp.bfloat16)
    route_grad = back_route[position].reshape(tok_rows, TOPK)
    return (
        token_grad,
        route_grad,
        grad_gate[None],
        grad_up[None],
        grad_down[None],
        gate_rows[None],
        up_rows[None],
        down_square[None],
    )


def solution(mesh):
    return jax.shard_map(
        on_device,
        mesh=mesh,
        in_specs=(
            P("ep", None),
            P("ep", None),
            P("ep", None),
            P("ep", None),
            P("ep", None, "tp"),
            P("ep", None, "tp"),
            P("ep", "tp", None),
        ),
        out_specs=(
            P("ep", "tp"),
            P("ep", None),
            P("ep", None, "tp"),
            P("ep", None, "tp"),
            P("ep", "tp", None),
            P("ep", None),
            P("ep", None),
            P("ep", "tp"),
        ),
        check_vma=False,
    )
```

profile of v0, /device:TPU:1, one launch (start us, length us, event | category | flops | bytes accessed | tf_op | source)
XLA Modules:
  0.0 218.1 jit_solution(3008970981896406860)
XLA Ops:
  7.2 0.7 broadcast_multiply_fusion
  8.0 0.8 copy.34
  8.8 0.8 copy.35
  10.4 1.4 scatter_custom_fusion
  11.8 2.2 scatter_custom_fusion.1
  14.2 1.0 constant_dynamic-slice_fusion
  15.3 2.0 gather_fusion
  17.4 2.0 gather_fusion.1
  20.1 51.7 %all_to_all.24 = bf16[128,4,1025]{2,1,0:T(4,128)(2,1)S(1)} all-to-all(bf16[128,4,1025]{2,1,0:T(4,128)(2,1)S(1)} %pad_maximum_fusion), channel_id=1, replica_groups=mesh['ep'=128,'tp'=4] {'ep'}, dimensions={0} | all-to-all | bytes 2099200 | tf_op jit(solution)/shard_map/all_to_all | solution.py:13
  72.4 1.0 pad_maximum_fusion.1
  73.9 47.0 %all-gather.2.cloned.1.call-done = bf16[1024,2048]{1,0:T(8,128)(2,1)} async-done(((bf16[1024,512]{1,0:T(8,128)(2,1)}), bf16[1024,2048]{1,0:T(8,128)(2,1)}) %all-gather.2.cloned.1.call-update) | async-done | bytes 4194320 | tf_op jit(solution)/shard_map/all_gather | solution.py:26
  120.9 2.6 %fusion.5 = f32[512,128]{0,1:T(8,128)S(1)} fusion(bf16[1024,2048]{1,0:T(8,128)(2,1)} %all-gather.2.cloned.1.call-done, bf16[1,2048,128]{2,1,0:T(8,128)(2,1)S(1)} %copy-done), kind=kOutput, calls=%fused_computation.15 | convolution fusion | flops 268435456 | bytes 2883584 | tf_op jit(solution)/shard_map/dot_general | solution.py:87
  123.5 2.5 %fusion.7 = f32[512,128]{0,1:T(8,128)S(1)} fusion(bf16[1024,2048]{1,0:T(8,128)(2,1)} %all-gather.2.cloned.1.call-done, bf16[1,2048,128]{2,1,0:T(8,128)(2,1)S(1)} %copy-done.1), kind=kOutput, calls=%fused_computation.17 | convolution fusion | flops 268435456 | bytes 2883584 | tf_op jit(solution)/shard_map/dot_general | solution.py:88
  126.0 0.9 multiply_reduce_fusion.3
  126.9 0.7 fusion.10
  127.7 2.1 add_convert_fusion
  129.8 2.0 multiply_reduce_fusion.2
  131.8 2.1 multiply_reduce_fusion.1
  134.0 7.4 %all_to_all.25 = f32[4,1,4608]{2,1,0:T(1,128)S(1)} all-to-all(f32[4,1,4608]{2,1,0:T(1,128)S(1)} %broadcast_in_dim.44), channel_id=1, replica_groups=mesh['ep'=128,'tp'=4] {'tp'}, dimensions={0} | all-to-all | bytes 147456 | tf_op jit(solution)/shard_map/all_to_all | solution.py:35
  141.7 23.8 %reduce-scatter.2.cloned.1.call-done = bf16[512,512]{1,0:T(8,128)(2,1)} async-done(((bf16[512,2048]{1,0:T(8,128)(2,1)}), bf16[512,512]{1,0:T(8,128)(2,1)}) %reduce-scatter.2.cloned.1.call-update) | async-done | bytes 524304 | tf_op jit(solution)/shard_map/reduce_scatter | solution.py:117
  165.5 1.2 concatenate.35
  166.6 1.2 pad_maximum_fusion.2
  167.8 14.3 %all-to-all-start.2 = ((bf16[128,4,513]{2,1,0:T(4,128)(2,1)}), bf16[128,4,513]{2,1,0:T(4,128)(2,1)S(1)}, u32[]{:S(2)}, u32[]{:S(2)}) async-start(bf16[128,4,513]{2,1,0:T(4,128)(2,1)} %pad_maximum_fusion.2), calls=%async_computation.3 | async-start | bytes 1310720 | tf_op jit(solution)/shard_map/all_to_all | solution.py:13
  182.2 1.0 copy.41
  183.2 1.0 copy.40
  184.2 3.4 %multiply_reduce_fusion = (f32[128]{0:T(128)}, bf16[128,2048]{1,0:T(8,128)(2,1)}) fusion(bf16[1024,2048]{1,0:T(8,128)(2,1)} %all-gather.2.cloned.1.call-done, f32[512]{0:T(512)S(1)} %convert_reduce_fusion, f32[512,128]{0,1:T(8,128)S(1)} %fusion.7, f32[512,128]{0,1:T(8,128)S(1)} %fusion.5), kind=kOutput, calls=%fused_computation.23 | convolution fusion | flops 269942656 | bytes 3148288 | tf_op jit(solution)/shard_map/dot_general | solution.py:102
  187.5 0.6 fusion.26
  188.1 17.3 %all-to-all-done.2 = bf16[128,4,513]{2,1,0:T(4,128)(2,1)S(1)} async-done(((bf16[128,4,513]{2,1,0:T(4,128)(2,1)}), bf16[128,4,513]{2,1,0:T(4,128)(2,1)S(1)}, u32[]{:S(2)}, u32[]{:S(2)}) %all-to-all-start.2) | async-done | bytes 525344 | tf_op jit(solution)/shard_map/all_to_all | solution.py:13
  206.0 1.2 gather_fusion.2
  207.1 1.9 gather_fusion.3
  209.2 1.3 reduce_sum.71
  210.7 0.6 copy.39
  (42 shorter events, 4.1 us)
Async XLA Ops:
  7.2 113.7 %copy-start = (bf16[1,2048,128]{2,1,0:T(8,128)(2,1)S(1)}, bf16[1,2048,128]{2,1,0:T(8,128)(2,1)}, u32[]{:S(2)}) copy-start(bf16[1,2048,128]{2,1,0:T(8,128)(2,1)} %param.11) | copy-start | bytes 1572868
  7.2 113.7 %all-gather.2.cloned.1.call-start = ((), (), s32[]{:S(2)}) async-start(), calls=%async_computation.4 | async-start | bytes 5242880 | tf_op jit(solution)/shard_map/all_gather | solution.py:26
  73.5 50.0 %copy-start.1 = (bf16[1,2048,128]{2,1,0:T(8,128)(2,1)S(1)}, bf16[1,2048,128]{2,1,0:T(8,128)(2,1)}, u32[]{:S(2)}) copy-start(bf16[1,2048,128]{2,1,0:T(8,128)(2,1)} %param.12) | copy-start | bytes 1572868
  73.5 91.9 %reduce-scatter.2.cloned.1.call-start = ((), (), s32[]{:S(2)}) async-start(), calls=%async_computation.5 | async-start | bytes 2621440 | tf_op jit(solution)/shard_map/reduce_scatter | solution.py:117
  120.9 5.1 %copy-start.2 = (bf16[1024,2048]{1,0:T(8,128)(2,1)S(1)}, bf16[1024,2048]{1,0:T(8,128)(2,1)}, u32[]{:S(2)}) copy-start(bf16[1024,2048]{1,0:T(8,128)(2,1)} %all-gather.2.cloned.1.call-done) | copy-start | bytes 12582916
  123.5 2.5 %copy-start.3 = (bf16[1,128,2048]{2,1,0:T(8,128)(2,1)S(1)}, bf16[1,128,2048]{2,1,0:T(8,128)(2,1)}, u32[]{:S(2)}) copy-start(bf16[1,128,2048]{2,1,0:T(8,128)(2,1)} %param.13) | copy-start | bytes 1572868
  167.8 37.7 %all-to-all-start.2 = ((bf16[128,4,513]{2,1,0:T(4,128)(2,1)}), bf16[128,4,513]{2,1,0:T(4,128)(2,1)S(1)}, u32[]{:S(2)}, u32[]{:S(2)}) async-start(bf16[128,4,513]{2,1,0:T(4,128)(2,1)} %pad_maximum_fusion.2), calls=%async_computation.3 | async-start | bytes 1310720 | tf_op jit(solution)/shard_map/all_to_all | solution.py:13
Sparse Core Ops, SparseCore 0:
  73.6 47.2 all-gather.1
  129.9 35.5 reduce-scatter.1
where the time goes:
time: 219 us; the launch traced here: 218 us
  waiting for transfers between devices  88.2 us (40%)
  blocking collectives  59.1 us (27%)
  local copies, waits for them, and re-layouts  20.3 us (9%)
  matrix products  16.5 us (8%)
  starting transfers between devices  14.6 us (7%)
  between operations  14.3 us (7%)
  other arithmetic  5.08 us (2%)
    all_to_all x1, blocking collectives, side_by_side(): lax.all_to_all(both, axis, split_axis=split_dim, concat_axis=concat_dim,...  51.7 us
    all_gather x1, waiting for transfers between devices, in_one_piece(): result, at, done = (lax.all_gather(both, axis, axis=dim, tiled=True), 0, [])  47 us
    reduce_scatter x1, waiting for transfers between devices, on_device(): lax.psum_scatter(token_term.astype(jnp.bfloat16), 'tp', scatter_dimension...  23.8 us
    all_to_all x1, waiting for transfers between devices, side_by_side(): lax.all_to_all(both, axis, split_axis=split_dim, concat_axis=concat_dim,...  17.3 us
    all_to_all x1, starting transfers between devices, side_by_side(): lax.all_to_all(both, axis, split_axis=split_dim, concat_axis=concat_dim,...  14.3 us
    all_to_all x1, blocking collectives, from_everyone(): lax.all_to_all(jnp.broadcast_to(shard[None], (count, *shard.shape)), axis...  7.38 us
  transfers between devices with their start and end apart: 3, of which 3 were waited for; matrix products, arithmetic and copies ran while one was open for 5% of the time, Pallas kernels for 0%

commit v1 on v0

v1 whole, which is shorter than its diff:
```python
import functools

import jax
import jax.numpy as jnp
from jax import lax
from jax.experimental import pallas as pl
from jax.experimental.pallas import tpu as pltpu
from jax.sharding import PartitionSpec as P

MESH = pl.DeviceIdType.MESH
BF = jnp.bfloat16
F32 = jnp.float32
I32 = jnp.int32

PLANES = 8
ROW = 16
GROUP = 32
TOK = 128
SEAT = 64
RELAY = 4 * SEAT
SLOTS = 512
BLK = 16
CH = 4
CW = 256
NN = (((1,), (0,)), ((), ()))
NT = (((1,), (1,)), ((), ()))
TN = (((0,), (0,)), ((), ()))


def mm(a, b, dims=NN, precision=None):
    return lax.dot_general(a, b, dims, precision=precision, preferred_element_type=F32)


def kernel(
    ids_ref, rw_ref, tok_hbm, cot_hbm, wg_hbm, wu_hbm, wd_hbm,
    tg_ref, rg_ref, gg_hbm, gu_hbm, gd_hbm, gr_ref, ur_ref, dr_ref,
    xc, t1, sendbuf, sendmeta, relay, zmeta, p2, pairbuf, scbuf, xs, scr,
    wgu, wdb, acc_gu, acc_hb, cot, whb, rp, rall, tt, sub_p, sub_m,
    s1p, s1m, dp, dm, s2p, s2m, ret, retr, back, backr, c01, c0, c1,
    tokbuf, rtb, srcv, srcr, ggb, gub, gdb, rnall,
    ld_s, w_s, z_s, z_r, zm_s, zm_r, y_s, y_r, ys_s, ys_r, x_s, x_r,
    r_s, r_r, s_s, s_r, b_s, b_r, br_s, br_r, zb_s, zb_r, zr_s, zr_r, n_s, n_r, g_s,
):
    ep = lax.axis_index("ep")
    t = lax.axis_index("tp")
    z = ep // ROW
    yc = ep % ROW
    sg = 1 - 2 * (z % 2)
    grp = z // 2
    base = grp * GROUP
    loc = ep % GROUP
    right = (t + 1) % 4
    left = (t + 3) % 4
    far = (t + 2) % 4

    def plane(off):
        return ((z + off + PLANES) % PLANES) * ROW + yc

    out_z = [plane(-sg), plane(2 * sg), plane(-3 * sg)]
    in_z = [plane(-sg), plane(-2 * sg), plane(-3 * sg)]

    def remote(src, dst, ssem, rsem, dev):
        return pltpu.make_async_remote_copy(
            src_ref=src, dst_ref=dst, send_sem=ssem, recv_sem=rsem,
            device_id=dev, device_id_type=MESH,
        )

    def drain(ref, sem):
        pltpu.make_async_copy(ref, ref, sem).wait()

    def peer(o):
        return (loc + o) % GROUP

    def rows16(i):
        return pl.ds(pl.multiple_of(i * BLK, BLK), BLK)

    def seat(i):
        return pl.ds(pl.multiple_of(i * SEAT, SEAT), SEAT)

    cols = pl.ds(pl.multiple_of(t * 512, 512), 512)
    ld = [
        pltpu.make_async_copy(tok_hbm.at[:, cols], xc.at[:, pl.ds(0, 512)], ld_s.at[0]),
        pltpu.make_async_copy(cot_hbm.at[:, cols], xc.at[:, pl.ds(512, 512)], ld_s.at[1]),
    ]
    wl = [
        pltpu.make_async_copy(wg_hbm, wgu.at[:, pl.ds(0, 128)], w_s.at[0]),
        pltpu.make_async_copy(wu_hbm, wgu.at[:, pl.ds(128, 128)], w_s.at[1]),
    ]
    for j in range(8):
        wl.append(pltpu.make_async_copy(wd_hbm.at[:, pl.ds(j * CW, CW)], wdb.at[j], w_s.at[2 + j]))
    for c in ld:
        c.start()
    for c in wl:
        c.start()

    barrier = pltpu.get_barrier_semaphore()

    def hello(e, k):
        pl.semaphore_signal(barrier, inc=1, device_id=(e, k), device_id_type=MESH)

    for k in (right, left, far):
        hello(ep, k)
    for e in (plane(-sg), plane(2), plane(-2), plane(-3 * sg)):
        hello(e, t)

    def hello_group(o, carry):
        hello(base + peer(o), t)
        return carry

    lax.fori_loop(1, GROUP, hello_group, 0)

    ids = ids_ref[...]
    id0, id1 = ids[0:1, :], ids[1:2, :]
    sub = lax.broadcasted_iota(I32, (TOK, TOK), 0)
    lane = lax.broadcasted_iota(I32, (TOK, TOK), 1)
    oh0 = jnp.where(sub == id0, 1.0, 0.0)
    oh1 = jnp.where(sub == id1, 1.0, 0.0)
    upper = jnp.where(sub < lane, 1.0, 0.0).astype(BF)
    before = mm((oh0 + oh1).astype(BF), upper)
    k0 = jnp.sum(before * oh0, axis=0, keepdims=True)
    k1 = jnp.sum(before * oh1, axis=0, keepdims=True)
    g = id0 // GROUP
    ohg = jnp.where(lax.broadcasted_iota(I32, (16, TOK), 0) == g, 1.0, 0.0)
    q = jnp.sum(mm(ohg.astype(BF), upper) * ohg, axis=0, keepdims=True)
    slot = g * SEAT + q.astype(I32)
    code0 = ((id0 - g * GROUP) * 4).astype(F32) + k0
    code1 = ((id1 - g * GROUP) * 4).astype(F32) + k1
    rw = rw_ref[...].astype(F32)
    mrow = jnp.where(
        sub == 0, code0,
        jnp.where(sub == 1, code1, jnp.where(sub == 2, rw[0:1, :], jnp.where(sub == 3, rw[1:2, :], 0.0))),
    ).astype(BF)
    t1[...] = jnp.where(lax.broadcasted_iota(I32, (RELAY, TOK), 0) == slot, 1.0, 0.0).astype(BF)
    sendmeta[...] = mm(t1[...], mrow, NT).astype(BF)
    for c in ld:
        c.wait()
    for h in range(CH):
        sendbuf[h] = mm(t1[...], xc[:, h * CW : (h + 1) * CW]).astype(BF)

    pl.semaphore_wait(barrier, 3 + 4 + GROUP - 1)

    for d in (1, 2, 3):
        dst = out_z[d - 1]
        seats = seat(dst // GROUP)
        here = pl.ds(d * SEAT, SEAT)
        remote(sendmeta.at[seats], zmeta.at[here], zm_s, zm_r, (dst, t)).start()
    for h in range(CH):
        for d in (1, 2, 3):
            dst = out_z[d - 1]
            seats = seat(dst // GROUP)
            here = pl.ds(d * SEAT, SEAT)
            remote(sendbuf.at[h, seats], relay.at[h, here], z_s.at[h], z_r.at[h], (dst, t)).start()
    zmeta[0:SEAT, :] = sendmeta[seat(grp), :]
    for h in range(CH):
        relay[h, 0:SEAT, :] = sendbuf[h, seat(grp), :]

    for c in wl:
        c.wait()

    drain(zmeta.at[pl.ds(SEAT, 3 * SEAT)], zm_r)
    pick = jnp.where(
        lax.broadcasted_iota(I32, (16, 128), 0) == lax.broadcasted_iota(I32, (16, 128), 1), 1.0, 0.0
    ).astype(BF)
    flat = mm(pick, zmeta[...], NT)
    seatrow = lax.broadcasted_iota(I32, (1, RELAY), 1) // SEAT

    def place(code, where_seat):
        code = code.astype(I32)
        return (code // 4) * BLK + where_seat * 4 + code % 4

    pos0 = place(flat[0:1, :], seatrow)
    pos1 = place(flat[1:2, :], seatrow)
    w0, w1 = flat[2:3, :], flat[3:4, :]
    ones256 = jnp.ones((RELAY, 128), BF)

    def spread(i, carry):
        at = pl.ds(pl.multiple_of(i * 128, 128), 128)
        p = lax.broadcasted_iota(I32, (128, RELAY), 0) + i * 128
        e0, e1 = p == pos0, p == pos1
        p2[at, :] = jnp.where(e0, 1.0, jnp.where(e1, 1.0, 0.0)).astype(BF)
        weights = (jnp.where(e0, w0, 0.0) + jnp.where(e1, w1, 0.0)).astype(BF)
        scbuf[at, :] = mm(weights, ones256).astype(BF)
        return carry

    lax.fori_loop(0, 4, spread, 0)

    def send_group(src, dst, ssem, rsem):
        def body(o, carry):
            e = peer(o)
            remote(src.at[rows16(e)], dst.at[rows16(loc)], ssem, rsem, (base + e, t)).start()
            return carry

        lax.fori_loop(1, GROUP, body, 0)

    mine = rows16(loc)
    most = pl.ds(0, (GROUP - 1) * BLK)

    def relay_step(h):
        drain(relay.at[h, pl.ds(SEAT, 3 * SEAT)], z_r.at[h])
        pairbuf[h] = mm(p2[...], relay[h]).astype(BF)
        send_group(pairbuf.at[h], xs.at[t, h], y_s.at[h], y_r.at[h])
        xs[t, h, mine, :] = pairbuf[h, mine, :]

    half0, half1 = pl.ds(0, 256), pl.ds(256, 256)

    def x_copies(h):
        return (
            remote(xs.at[t, h], xs.at[t, h], x_s.at[h, 0], x_r.at[h, 0], (ep, right)),
            remote(xs.at[t, h], xs.at[t, h], x_s.at[h, 1], x_r.at[h, 1], (ep, left)),
        )

    def f_copies(h):
        return (
            remote(xs.at[left, h, half0], xs.at[left, h, half0], x_s.at[h, 2], x_r.at[h, 2], (ep, right)),
            remote(xs.at[right, h, half1], xs.at[right, h, half1], x_s.at[h, 3], x_r.at[h, 3], (ep, left)),
        )

    def gather_step(h):
        drain(pairbuf.at[h, most], y_r.at[h])
        for c in x_copies(h):
            c.start()

    def forward_step(h):
        for c in x_copies(h):
            c.wait_recv()
        for c in f_copies(h):
            c.start()

    def arrive_step(h):
        for c in f_copies(h):
            c.wait_recv()

    def product(k, h, first=False):
        if h < 2:
            at = pl.ds(pl.multiple_of(k * 512 + h * CW, CW), CW)
            part = mm(xs[k, h], wgu[at, :])
            if first:
                acc_gu[...] = part
            else:
                acc_gu[...] += part
        else:
            part = mm(xs[k, h], wdb[k * 2 + (h - 2)], NT)
            if first:
                acc_hb[...] = part
            else:
                acc_hb[...] += part

    def near_products(h):
        product(t, h, first=(h % 2 == 0))

        def body(i, carry):
            product((t + 1 + 2 * i) % 4, h)
            return carry

        lax.fori_loop(0, 2, body, 0)

    relay_step(0)
    send_group(scbuf, scr, ys_s, ys_r)
    scr[mine, :] = scbuf[mine, :]
    relay_step(1)
    relay_step(2)
    gather_step(0)
    relay_step(3)
    gather_step(1)
    forward_step(0)
    near_products(0)

    seatcol = lax.broadcasted_iota(I32, (RELAY, 1), 0) // SEAT
    codes = zmeta[...].astype(F32)
    back0 = place(codes[:, 0:1], seatcol)
    back1 = place(codes[:, 1:2], seatcol)
    wide = lax.broadcasted_iota(I32, (RELAY, SLOTS), 1)
    m0 = jnp.where(wide == back0, 1.0, 0.0)
    m1 = jnp.where(wide == back1, 1.0, 0.0)
    c0[...] = m0.astype(BF)
    c1[...] = m1.astype(BF)
    c01[...] = (m0 + m1).astype(BF)

    gather_step(2)
    forward_step(1)
    near_products(1)
    gather_step(3)
    forward_step(2)
    near_products(2)
    arrive_step(0)
    product(far, 0)
    arrive_step(1)
    product(far, 1)
    forward_step(3)
    near_products(3)
    arrive_step(2)
    product(far, 2)
    drain(scbuf.at[most], ys_r)
    arrive_step(3)
    product(far, 3)

    def activate(i, carry):
        at = pl.ds(pl.multiple_of(i * 64, 64), 64)
        gate, up = acc_gu[at, 0:128], acc_gu[at, 128:256]
        hb = acc_hb[at, :]
        sc = scr[at, :].astype(F32)
        sig = jax.nn.sigmoid(gate)
        act = gate * sig
        hid = act * up
        hc = sc * hb
        cot[at, 0:128] = (hc * up * sig * (1.0 + gate * (1.0 - sig))).astype(BF)
        cot[at, 128:256] = (hc * act).astype(BF)
        whb[at, :] = (sc * hid).astype(BF)
        rp[at, :] = hid * hb
        return carry

    lax.fori_loop(0, 8, activate, 0)

    def share(k, p):
        at = pl.ds(pl.multiple_of(k * 512 + p * CW, CW), CW)
        part = mm(cot[...], wgu[at, :], NT).astype(BF)
        tt[k, 2 * p] = part[:, 0:128]
        tt[k, 2 * p + 1] = part[:, 128:256]

    def s1_copies(p):
        return (
            remote(tt.at[far, 2 * p], s1p.at[p], s_s.at[p, 0], s_r.at[p, 0], (ep, right)),
            remote(tt.at[far, 2 * p + 1], s1m.at[p], s_s.at[p, 1], s_r.at[p, 1], (ep, left)),
        )

    def d_copies(p):
        return (
            remote(tt.at[right, 2 * p + 1], dp.at[p], s_s.at[p, 2], s_r.at[p, 2], (ep, right)),
            remote(tt.at[left, 2 * p], dm.at[p], s_s.at[p, 3], s_r.at[p, 3], (ep, left)),
        )

    def s2_copies(p):
        return (
            remote(sub_p.at[p], s2p.at[p], s_s.at[p, 4], s_r.at[p, 4], (ep, right)),
            remote(sub_m.at[p], s2m.at[p], s_s.at[p, 5], s_r.at[p, 5], (ep, left)),
        )

    def everyone(buf, ssem, rsem):
        return [
            remote(buf.at[t], buf.at[t], ssem.at[i], rsem.at[i], (ep, k))
            for i, k in enumerate((right, left, far))
        ]

    share(far, 0)
    for c in s1_copies(0):
        c.start()
    share(right, 0)
    share(left, 0)
    for c in d_copies(0):
        c.start()

    ones16 = jnp.ones((16, 128), F32)
    rsum = mm(ones16, rp[...], NT, lax.Precision.HIGHEST)
    rall[t] = rsum[0:8, :]
    share(far, 1)
    share(right, 1)
    share(left, 1)
    r_copies = everyone(rall, r_s, r_r)
    for c in r_copies:
        c.start()
    share(t, 0)
    share(t, 1)

    def second(p):
        for c in s1_copies(p):
            c.wait_recv()
        sub_p[p] = (s1p[p].astype(F32) + tt[right, 2 * p].astype(F32)).astype(BF)
        sub_m[p] = (s1m[p].astype(F32) + tt[left, 2 * p + 1].astype(F32)).astype(BF)
        for c in s2_copies(p):
            c.start()

    def reduced(p):
        for c in (*s2_copies(p), *d_copies(p)):
            c.wait_recv()
        ret[p, :, 0:128] = (
            tt[t, 2 * p].astype(F32) + s2p[p].astype(F32) + dm[p].astype(F32)
        ).astype(BF)
        ret[p, :, 128:256] = (
            tt[t, 2 * p + 1].astype(F32) + s2m[p].astype(F32) + dp[p].astype(F32)
        ).astype(BF)
        send_group(ret.at[p], back.at[p], b_s.at[p], b_r.at[p])
        back[p, mine, :] = ret[p, mine, :]

    ones8 = jnp.ones((16, 128), F32)

    def wgrad(j):
        k, h = j // 2, j % 2
        d0 = pl.multiple_of(j * CW, CW)
        at = pl.ds(d0, CW)
        both = mm(xs[k, h], cot[...], TN).astype(BF)
        ggb[at, :] = both[:, 0:128]
        gub[at, :] = both[:, 128:256]
        sq = jnp.square(both.astype(F32))
        ng = mm(ones8, sq[:, 0:128], NT, lax.Precision.HIGHEST)
        nu = mm(ones8, sq[:, 128:256], NT, lax.Precision.HIGHEST)
        rnall[t, pl.ds(2 * j, 1), :] = ng[0:1, 0:128]
        rnall[t, pl.ds(2 * j + 1, 1), :] = ng[0:1, 128:256]
        rnall[t, pl.ds(16 + 2 * j, 1), :] = nu[0:1, 0:128]
        rnall[t, pl.ds(17 + 2 * j, 1), :] = nu[0:1, 128:256]

    def dgrad(j, total):
        k, h = j // 2, j % 2
        down = mm(whb[...], xs[k, 2 + h], TN).astype(BF)
        gdb[j] = down
        sq = jnp.square(down.astype(F32))
        return total + sq[:, 0:128] + sq[:, 128:256]

    def wgrads(lo, hi):
        def body(j, carry):
            wgrad(j)
            return carry

        lax.fori_loop(lo, hi, body, 0)

    wgrads(0, 4)
    second(0)
    for c in s1_copies(1):
        c.start()
    for c in d_copies(1):
        c.start()
    wgrads(4, 8)
    n_copies = everyone(rnall, n_s, n_r)
    for c in n_copies:
        c.start()
    gcopies = [
        pltpu.make_async_copy(ggb, gg_hbm, g_s.at[0]),
        pltpu.make_async_copy(gub, gu_hbm, g_s.at[1]),
    ]
    for c in gcopies:
        c.start()

    for c in r_copies:
        c.wait_recv()
    rtot = ((rall[0] + rall[1]) + rall[2]) + rall[3]
    rtot = jnp.where(lax.broadcasted_iota(I32, (8, SLOTS), 0) == 0, rtot, 0.0)
    retr[...] = mm(rtot.astype(BF), jnp.ones((8, 128), BF), TN).astype(BF)
    reduced(0)
    send_group(retr, backr, br_s, br_r)
    backr[mine, :] = retr[mine, :]
    second(1)

    total = lax.fori_loop(0, 8, dgrad, jnp.zeros((128, 128), F32))
    dcopies = [
        pltpu.make_async_copy(gdb.at[j], gd_hbm.at[:, pl.ds(j * CW, CW)], g_s.at[2 + j])
        for j in range(8)
    ]
    for c in dcopies:
        c.start()
    dr_ref[...] = mm(ones16, total, NT, lax.Precision.HIGHEST)[0:1, :]

    def home(src, dst, ssem, rsem):
        for d in (1, 2, 3):
            remote(src.at[pl.ds(d * SEAT, SEAT)], dst.at[seat(grp)], ssem, rsem, (in_z[d - 1], t)).start()

    def combine(p):
        drain(ret.at[p, most], b_r.at[p])
        tokbuf[p] = mm(c01[...], back[p]).astype(BF)
        home(tokbuf.at[p], srcv.at[p], zb_s.at[p], zb_r.at[p])
        srcv[p, seat(grp), :] = tokbuf[p, 0:SEAT, :]

    reduced(1)
    combine(0)
    drain(retr.at[most], br_r)
    lane2 = lax.broadcasted_iota(I32, (RELAY, 128), 1)
    rtb[...] = jnp.where(lane2 == 0, mm(c0[...], backr[...]), mm(c1[...], backr[...])).astype(BF)
    home(rtb, srcr, zr_s, zr_r)
    srcr[seat(grp), :] = rtb[0:SEAT, :]

    for c in n_copies:
        c.wait_recv()
    norms = ((rnall[0] + rnall[1]) + rnall[2]) + rnall[3]
    gr_ref[...] = norms[0:16, :]
    ur_ref[...] = norms[16:32, :]
    combine(1)

    three = pl.ds(0, 3 * SEAT)
    drain(tokbuf.at[0, three], zb_r.at[0])
    tg_ref[:, 0:256] = mm(t1[...], srcv[0], TN).astype(BF)
    drain(rtb.at[three], zr_r)
    rg_ref[...] = mm(srcr[...], t1[...], TN)[0:2, :].astype(BF)

    drain(sendmeta.at[three], zm_s)
    for h in range(CH):
        drain(sendbuf.at[h, three], z_s.at[h])
        drain(pairbuf.at[h, most], y_s.at[h])
        for c in (*x_copies(h), *f_copies(h)):
            c.wait_send()
    drain(scbuf.at[most], ys_s)
    for c in (*r_copies, *n_copies):
        c.wait_send()
    for p in range(2):
        for c in (*s1_copies(p), *d_copies(p), *s2_copies(p)):
            c.wait_send()
        drain(ret.at[p, most], b_s.at[p])
        drain(tokbuf.at[p, three], zb_s.at[p])
    drain(retr.at[most], br_s)
    drain(rtb.at[three], zr_s)
    for c in (*gcopies, *dcopies):
        c.wait()
    drain(tokbuf.at[1, three], zb_r.at[1])
    tg_ref[:, 256:512] = mm(t1[...], srcv[1], TN).astype(BF)


def on_device(tokens, expert_ids, route_weights, cotangent, w_gate, w_up, w_down):
    vmem = pl.BlockSpec(memory_space=pltpu.VMEM)
    hbm = pl.BlockSpec(memory_space=pl.ANY)
    dma = pltpu.SemaphoreType.DMA
    v = pltpu.VMEM
    scratch = [
        v((TOK, 1024), BF),
        v((RELAY, TOK), BF),
        v((CH, RELAY, CW), BF),
        v((RELAY, 128), BF),
        v((CH, RELAY, CW), BF),
        v((RELAY, 128), BF),
        v((SLOTS, RELAY), BF),
        v((CH, SLOTS, CW), BF),
        v((SLOTS, 128), BF),
        v((4, CH, SLOTS, CW), BF),
        v((SLOTS, 128), BF),
        v((2048, 256), BF),
        v((8, 128, CW), BF),
        v((SLOTS, 256), F32),
        v((SLOTS, 128), F32),
        v((SLOTS, 256), BF),
        v((SLOTS, 128), BF),
        v((SLOTS, 128), F32),
        v((4, 8, SLOTS), F32),
        v((4, 4, SLOTS, 128), BF),
        v((2, SLOTS, 128), BF),
        v((2, SLOTS, 128), BF),
        v((2, SLOTS, 128), BF),
        v((2, SLOTS, 128), BF),
        v((2, SLOTS, 128), BF),
        v((2, SLOTS, 128), BF),
        v((2, SLOTS, 128), BF),
        v((2, SLOTS, 128), BF),
        v((2, SLOTS, CW), BF),
        v((SLOTS, 128), BF),
        v((2, SLOTS, CW), BF),
        v((SLOTS, 128), BF),
        v((RELAY, SLOTS), BF),
        v((RELAY, SLOTS), BF),
        v((RELAY, SLOTS), BF),
        v((2, RELAY, CW), BF),
        v((RELAY, 128), BF),
        v((2, RELAY, CW), BF),
        v((RELAY, 128), BF),
        v((2048, 128), BF),
        v((2048, 128), BF),
        v((8, 128, CW), BF),
        v((4, 32, 128), F32),
        dma((2,)), dma((10,)),
        dma((CH,)), dma((CH,)), dma(()), dma(()),
        dma((CH,)), dma((CH,)), dma(()), dma(()),
        dma((CH, 4)), dma((CH, 4)),
        dma((3,)), dma((3,)),
        dma((2, 6)), dma((2, 6)),
        dma((2,)), dma((2,)), dma(()), dma(()),
        dma((2,)), dma((2,)), dma(()), dma(()),
        dma((3,)), dma((3,)), dma((10,)),
    ]
    s = jax.ShapeDtypeStruct
    tg, rg, gg, gu, gd, gr, ur, dr = pl.pallas_call(
        kernel,
        out_shape=(
            s((TOK, 512), BF), s((2, TOK), BF), s((2048, 128), BF), s((2048, 128), BF),
            s((128, 2048), BF), s((16, 128), F32), s((16, 128), F32), s((1, 128), F32),
        ),
        in_specs=[vmem, vmem, hbm, hbm, hbm, hbm, hbm],
        out_specs=(vmem, vmem, hbm, hbm, hbm, vmem, vmem, vmem),
        scratch_shapes=scratch,
        compiler_params=pltpu.CompilerParams(collective_id=0, has_side_effects=True),
    )(expert_ids.T, route_weights.T, tokens, cotangent, w_gate[0], w_up[0], w_down[0])
    return (
        tg, rg.T, gg[None], gu[None], gd[None],
        gr.reshape(1, 2048), ur.reshape(1, 2048), dr,
    )


def solution(mesh):
    return jax.shard_map(
        on_device,
        mesh=mesh,
        in_specs=(
            P("ep", None), P("ep", None), P("ep", None), P("ep", None),
            P("ep", None, "tp"), P("ep", None, "tp"), P("ep", "tp", None),
        ),
        out_specs=(
            P("ep", "tp"), P("ep", None), P("ep", None, "tp"), P("ep", None, "tp"),
            P("ep", "tp", None), P("ep", None), P("ep", None), P("ep", "tp"),
        ),
        check_vma=False,
    )
```

time: 219 us -> 122 us (0.56)
  Pallas kernels: 0 us -> 113 us
  waiting for transfers between devices: 88.2 us -> 0 us
  blocking collectives: 59.1 us -> 0 us
  matrix products: 16.5 us -> 0 us
  starting transfers between devices: 14.6 us -> 0 us
  between operations: 14.3 us -> 0.66 us
  local copies, waits for them, and re-layouts: 20.3 us -> 7.93 us
  other arithmetic: 5.08 us -> 0 us
    pallas_call x0 -> x1, Pallas kernels: none -> 113 us  [on_device(): pl.pallas_call(kernel, out_shape=(s((TOK, 512), BF), s((2, TOK), BF), s((...]
    all_to_all x2 -> x0, blocking collectives: 59.1 us -> none  [the longest x1 51.7 us: side_by_side(): lax.all_to_all(both, axis, split_axis=split_dim, concat_axis=concat_dim,...]
    all_gather x1 -> x0, waiting for transfers between devices: 47 us -> none  [in_one_piece(): result, at, done = (lax.all_gather(both, axis, axis=dim, tiled=True), 0, [])]
    reduce_scatter x1 -> x0, waiting for transfers between devices: 23.8 us -> none  [on_device(): lax.psum_scatter(token_term.astype(jnp.bfloat16), 'tp', scatter_dimension...]
    all_to_all x1 -> x0, waiting for transfers between devices: 17.3 us -> none  [side_by_side(): lax.all_to_all(both, axis, split_axis=split_dim, concat_axis=concat_dim,...]
    dot_general x9 -> x0, matrix products: 16.5 us -> none  [the longest x1 3.36 us: on_device(): lax.dot_general(weighted_hidden, slot_cot, (((0,), (0,)), ((), ())), pref...]
    all_to_all x1 -> x0, starting transfers between devices: 14.3 us -> none  [side_by_side(): lax.all_to_all(both, axis, split_axis=split_dim, concat_axis=concat_dim,...]
    gather x5 -> x0, local copies, waits for them, and re-layouts: 7.13 us -> none  [the longest x1 1.97 us: on_device(): outgoing = rows_pad[slot_owner]]
  transfers between devices with their start and end apart: 3 -> 0, of which waited for: 3 -> 0; matrix products, arithmetic and copies ran while one was open for 5% -> 0% of each run, Pallas kernels for 0% -> 0%
where the time goes in v1:
time: 122 us
  Pallas kernels  113 us (93%)
  local copies, waits for them, and re-layouts  7.93 us (6%)
    pallas_call x1, Pallas kernels, on_device(): pl.pallas_call(kernel, out_shape=(s((TOK, 512), BF), s((2, TOK), BF), s((...  113 us
    unnamed x20, local copies, waits for them, and re-layouts  7.93 us

profile of v1, /device:TPU:1, one launch (start us, length us, event | category | flops | bytes accessed | tf_op | source)
XLA Modules:
  0.0 122.1 jit_solution(10092632132352335018)
XLA Ops:
  0.6 113.5 %shard_map.134 = (bf16[128,512]{1,0:T(8,128)(2,1)}, bf16[2,128]{1,0:T(2,128)(2,1)}, bf16[2048,128]{1,0:T(8,128)(2,1)}, bf16[2048,128]{1,0:T(8,128)(2,1)}, bf16[1...) custom-call(s32[2,128]{1,0:T(2,128)} %bitcast.19, bf16[2,128]{1,0:T(2,128)(2,1)} %bitcast.20, ...), custom_call_target="tpu_custom_call" | custom-call | tf_op jit(solution)/shard_map/pallas_call | solution.py:564
  114.1 0.0 copy-start.5
  114.1 1.6 %copy.23 = bf16[128,512]{1,0:T(8,128)(2,1)} copy(bf16[128,512]{1,0:T(8,128)(2,1)} %get-tuple-element.32) | data formatting | bytes 262144
  115.7 0.0 copy-done.5
  115.7 0.5 copy.24
  116.2 0.0 copy-start.1
  116.2 1.9 %copy.25 = bf16[1,2048,128]{2,1,0:T(8,128)(2,1)} copy(bf16[1,2048,128]{2,1,0:T(8,128)(2,1)} %bitcast.13) | data formatting | bytes 1048576
  118.2 0.0 copy-done.1
  118.2 0.0 copy-start
  118.2 0.8 copy.26
  119.0 0.4 copy-done
  119.4 0.0 copy-start.3
  119.4 0.8 copy.27
  120.2 0.0 copy-done.3
  120.2 0.0 copy-start.2
  120.2 0.6 copy.28
  120.8 0.1 copy-done.2
  120.9 0.0 copy-start.4
  120.9 0.6 copy.29
  121.5 0.1 copy-done.4
  121.6 0.5 copy.30
Async XLA Ops:
  114.1 1.6 %copy-start.5 = (bf16[2,128]{1,0:T(2,128)(2,1)S(1)}, bf16[2,128]{1,0:T(2,128)(2,1)}, u32[]{:S(2)}) copy-start(bf16[2,128]{1,0:T(2,128)(2,1)} %get-tuple-element.17) | copy-start | bytes 1540
  116.2 1.9 %copy-start.1 = (bf16[2048,128]{1,0:T(8,128)(2,1)S(1)}, bf16[2048,128]{1,0:T(8,128)(2,1)}, u32[]{:S(2)}) copy-start(bf16[2048,128]{1,0:T(8,128)(2,1)} %get-tuple-element.19) | copy-start | bytes 1572868
  118.2 1.2 %copy-start = (bf16[128,2048]{1,0:T(8,128)(2,1)S(1)}, bf16[128,2048]{1,0:T(8,128)(2,1)}, u32[]{:S(2)}) copy-start(bf16[128,2048]{1,0:T(8,128)(2,1)} %get-tuple-element.20) | copy-start | bytes 1572868
  119.4 0.8 copy-start.3
  120.2 0.7 copy-start.2
  120.9 0.7 copy-start.4

commit v2 on v1

v2 whole, which is shorter than its diff:
```python
import functools

import jax
import jax.numpy as jnp
from jax import lax
from jax.experimental import pallas as pl
from jax.experimental.pallas import tpu as pltpu
from jax.sharding import PartitionSpec as P

MESH = pl.DeviceIdType.MESH
BF = jnp.bfloat16
F32 = jnp.float32
I32 = jnp.int32

PLANES = 8
ROW = 16
GROUP = 32
TOK = 128
SEAT = 64
RELAY = 4 * SEAT
SLOTS = 512
BLK = 16
CHUNKS = ((0, 1), (1, 1), (2, 1), (3, 1), (4, 2), (6, 2))
NN = (((1,), (0,)), ((), ()))
NT = (((1,), (1,)), ((), ()))
TN = (((0,), (0,)), ((), ()))


def mm(a, b, dims=NN, precision=None):
    return lax.dot_general(a, b, dims, precision=precision, preferred_element_type=F32)


def kernel(
    ids_hbm, rw_hbm, tok_hbm, cot_hbm, wg_hbm, wu_hbm, wd_hbm,
    tg_ref, rg_ref, ggb, gub, gdr, gr_ref, ur_ref, dr_ref,
    xc, t1, sendbuf, sendmeta, relay, zmeta, p2, pairbuf, scbuf, xs, cs, scr,
    wgu, wdd, acc_gu, acc_hb, cot, wha, rp, rall, tt, sub_p, sub_m,
    s1p, s1m, dp, dm, s2p, s2m, ret, retr, back, backr, c01, c0, c1,
    tokbuf, rtb, srcv, srcr, gds, gdin, rnall, ids_v, rw_v,
    ld_s, w_s, z_s, z_r, zm_s, zm_r, y_s, y_r, ys_s, ys_r, x_s, x_r, h_s, h_r, v_s, v_r, e_s, e_r,
    r_s, r_r, s_s, s_r, b_s, b_r, br_s, br_r, zb_s, zb_r, zr_s, zr_r, n_s, n_r,
):
    ep = lax.axis_index("ep")
    t = lax.axis_index("tp")
    z = ep // ROW
    yc = ep % ROW
    sg = 1 - 2 * (z % 2)
    grp = z // 2
    base = grp * GROUP
    loc = ep % GROUP
    right = (t + 1) % 4
    left = (t + 3) % 4
    far = (t + 2) % 4

    def plane(off):
        return ((z + off + PLANES) % PLANES) * ROW + yc

    out_z = [plane(-sg), plane(2 * sg), plane(-3 * sg)]
    in_z = [plane(-sg), plane(-2 * sg), plane(-3 * sg)]

    def remote(src, dst, ssem, rsem, dev):
        return pltpu.make_async_remote_copy(
            src_ref=src, dst_ref=dst, send_sem=ssem, recv_sem=rsem,
            device_id=dev, device_id_type=MESH,
        )

    def drain(ref, sem):
        pltpu.make_async_copy(ref, ref, sem).wait()

    def begin(copies):
        for c in copies:
            c.start()

    def landed(copies):
        for c in copies:
            c.wait_recv()

    def left_here(copies):
        for c in copies:
            c.wait_send()

    def peer(o):
        return (loc + o) % GROUP

    def rows16(i):
        return pl.ds(pl.multiple_of(i * BLK, BLK), BLK)

    def seat(i):
        return pl.ds(pl.multiple_of(i * SEAT, SEAT), SEAT)

    def block(k):
        return pl.ds(pl.multiple_of(k * 512, 512), 512)

    route_in = [
        pltpu.make_async_copy(ids_hbm, ids_v, ld_s.at[2]),
        pltpu.make_async_copy(rw_hbm, rw_v, ld_s.at[3]),
    ]
    begin(route_in)
    ld = [
        pltpu.make_async_copy(tok_hbm.at[:, block(t)], xc.at[:, pl.ds(0, 512)], ld_s.at[0]),
        pltpu.make_async_copy(cot_hbm.at[:, block(t)], xc.at[:, pl.ds(512, 512)], ld_s.at[1]),
    ]
    wl = [
        pltpu.make_async_copy(wg_hbm, wgu.at[:, pl.ds(0, 128)], w_s.at[0]),
        pltpu.make_async_copy(wu_hbm, wgu.at[:, pl.ds(128, 128)], w_s.at[1]),
        pltpu.make_async_copy(wd_hbm.at[:, block(t)], wdd.at[t], w_s.at[2]),
    ]
    begin(ld)

    barrier = pltpu.get_barrier_semaphore()

    def hello(e, k):
        pl.semaphore_signal(barrier, inc=1, device_id=(e, k), device_id_type=MESH)

    for e in (plane(-3 * sg), plane(2), plane(-2), plane(-sg)):
        hello(e, t)
    for k in (far, right, left):
        hello(ep, k)

    def hello_group(o, carry):
        hello(base + peer(o), t)
        return carry

    lax.fori_loop(1, GROUP, hello_group, 0)

    for c in route_in:
        c.wait()
    ids = ids_v[...]
    id0, id1 = ids[0:1, :], ids[1:2, :]
    sub = lax.broadcasted_iota(I32, (TOK, TOK), 0)
    lane = lax.broadcasted_iota(I32, (TOK, TOK), 1)
    oh0 = jnp.where(sub == id0, 1.0, 0.0)
    oh1 = jnp.where(sub == id1, 1.0, 0.0)
    upper = jnp.where(sub < lane, 1.0, 0.0).astype(BF)
    before = mm((oh0 + oh1).astype(BF), upper)
    k0 = jnp.sum(before * oh0, axis=0, keepdims=True)
    k1 = jnp.sum(before * oh1, axis=0, keepdims=True)
    g = id0 // GROUP
    ohg = jnp.where(lax.broadcasted_iota(I32, (16, TOK), 0) == g, 1.0, 0.0)
    q = jnp.sum(mm(ohg.astype(BF), upper) * ohg, axis=0, keepdims=True)
    slot = g * SEAT + q.astype(I32)
    code0 = ((id0 - g * GROUP) * 4).astype(F32) + k0
    code1 = ((id1 - g * GROUP) * 4).astype(F32) + k1
    rw = rw_v[...].astype(F32)
    mrow = jnp.where(
        sub == 0, code0,
        jnp.where(sub == 1, code1, jnp.where(sub == 2, rw[0:1, :], jnp.where(sub == 3, rw[1:2, :], 0.0))),
    ).astype(BF)
    t1[...] = jnp.where(lax.broadcasted_iota(I32, (RELAY, TOK), 0) == slot, 1.0, 0.0).astype(BF)
    sendmeta[...] = mm(t1[...], mrow, NT).astype(BF)
    for c in ld:
        c.wait()
    for h in range(4):
        part = mm(t1[...], xc[:, h * 256 : (h + 1) * 256]).astype(BF)
        sendbuf[2 * h] = part[:, 0:128]
        sendbuf[2 * h + 1] = part[:, 128:256]

    pl.semaphore_wait(barrier, 3 + 4 + GROUP - 1)

    def send_meta():
        for d in (1, 2, 3):
            dst = out_z[d - 1]
            here = pl.ds(d * SEAT, SEAT)
            remote(sendmeta.at[seat(dst // GROUP)], zmeta.at[here], zm_s, zm_r, (dst, t)).start()

    def send_z(i):
        qs = pl.ds(*CHUNKS[i])
        for d in (1, 2, 3):
            dst = out_z[d - 1]
            here = pl.ds(d * SEAT, SEAT)
            remote(
                sendbuf.at[qs, seat(dst // GROUP)], relay.at[qs, here], z_s.at[i], z_r.at[i], (dst, t)
            ).start()

    exch = [
        remote(wd_hbm.at[:, block(k)], wdd.at[t], e_s.at[i], e_r.at[i], (ep, k))
        for i, k in enumerate((right, left, far))
    ]
    send_meta()
    send_z(0)
    send_z(1)
    begin(wl)
    begin(exch)
    zmeta[0:SEAT, :] = sendmeta[seat(grp), :]
    for h in range(8):
        relay[h, 0:SEAT, :] = sendbuf[h, seat(grp), :]

    drain(zmeta.at[pl.ds(SEAT, 3 * SEAT)], zm_r)
    send_z(2)
    pick = jnp.where(
        lax.broadcasted_iota(I32, (16, 128), 0) == lax.broadcasted_iota(I32, (16, 128), 1), 1.0, 0.0
    ).astype(BF)
    flat = mm(pick, zmeta[...], NT)
    seatrow = lax.broadcasted_iota(I32, (1, RELAY), 1) // SEAT

    def place(code, where_seat):
        code = code.astype(I32)
        return (code // 4) * BLK + where_seat * 4 + code % 4

    pos0 = place(flat[0:1, :], seatrow)
    pos1 = place(flat[1:2, :], seatrow)
    w0, w1 = flat[2:3, :], flat[3:4, :]
    ones256 = jnp.ones((RELAY, 128), BF)

    def spread(i, carry):
        at = pl.ds(pl.multiple_of(i * 128, 128), 128)
        p = lax.broadcasted_iota(I32, (128, RELAY), 0) + i * 128
        e0, e1 = p == pos0, p == pos1
        p2[at, :] = jnp.where(e0, 1.0, jnp.where(e1, 1.0, 0.0)).astype(BF)
        weights = (jnp.where(e0, w0, 0.0) + jnp.where(e1, w1, 0.0)).astype(BF)
        scbuf[at, :] = mm(weights, ones256).astype(BF)
        return carry

    lax.fori_loop(0, 4, spread, 0)

    def send_group(src, dst, ssem, rsem):
        def body(o, carry):
            e = peer(o)
            remote(src(rows16(e)), dst(rows16(loc)), ssem, rsem, (base + e, t)).start()
            return carry

        lax.fori_loop(1, GROUP, body, 0)

    mine = rows16(loc)
    most = pl.ds(0, (GROUP - 1) * BLK)

    def relay_step(i):
        q0, n = CHUNKS[i]
        drain(relay.at[pl.ds(q0, n), pl.ds(SEAT, 3 * SEAT)], z_r.at[i])
        rows = relay[q0] if n == 1 else jnp.concatenate([relay[q0], relay[q0 + 1]], axis=1)
        out = mm(p2[...], rows).astype(BF)
        for k in range(n):
            pairbuf[q0 + k] = out[:, k * 128 : (k + 1) * 128]
        qs = pl.ds(q0, n)
        if q0 < 4:
            send_group(
                lambda r: pairbuf.at[qs, r], lambda r: xs.at[t, qs, r], y_s.at[i], y_r.at[i]
            )
            for k in range(n):
                xs[t, q0 + k, mine, :] = pairbuf[q0 + k, mine, :]
        else:
            qc = pl.ds(q0 - 4, n)
            send_group(
                lambda r: pairbuf.at[qs, r], lambda r: cs.at[qc, r], y_s.at[i], y_r.at[i]
            )
            for k in range(n):
                cs[q0 - 4 + k, mine, :] = pairbuf[q0 + k, mine, :]

    def routed(i):
        drain(pairbuf.at[pl.ds(*CHUNKS[i]), most], y_r.at[i])

    half0, half1 = pl.ds(0, 256), pl.ds(256, 256)

    def x_copies(i):
        qs = pl.ds(*CHUNKS[i])
        return (
            remote(xs.at[t, qs], xs.at[t, qs], x_s.at[i, 0], x_r.at[i, 0], (ep, right)),
            remote(xs.at[t, qs], xs.at[t, qs], x_s.at[i, 1], x_r.at[i, 1], (ep, left)),
        )

    def f_copies(i):
        qs = pl.ds(*CHUNKS[i])
        return (
            remote(xs.at[left, qs, half0], xs.at[left, qs, half0], x_s.at[i, 2], x_r.at[i, 2], (ep, right)),
            remote(xs.at[right, qs, half1], xs.at[right, qs, half1], x_s.at[i, 3], x_r.at[i, 3], (ep, left)),
        )

    def forward_step(i):
        landed(x_copies(i))
        begin(f_copies(i))

    def product(k, i, first=False):
        q0, n = CHUNKS[i]
        at = pl.ds(pl.multiple_of(k * 512 + q0 * 128, 128), n * 128)
        rows = xs[k, q0] if n == 1 else jnp.concatenate([xs[k, q0], xs[k, q0 + 1]], axis=1)
        part = mm(rows, wgu[at, :])
        if first:
            acc_gu[...] = part
        else:
            acc_gu[...] += part

    def near_products(i):
        def body(j, carry):
            product((t + 1 + 2 * j) % 4, i)
            return carry

        lax.fori_loop(0, 2, body, 0)

    def hb_part(c, first):
        rows = jnp.concatenate([cs[2 * c], cs[2 * c + 1]], axis=1)

        def body(k, carry):
            part = mm(rows, wdd[k, :, c * 256 : (c + 1) * 256], NT)
            if first:
                acc_hb[k] = part
            else:
                tt[k, 4] = (acc_hb[k] + part).astype(BF)
            return carry

        lax.fori_loop(0, 4, body, 0)

    def s1_copies(p):
        return (
            remote(tt.at[far, p, half0], s1p.at[p], s_s.at[p, 0], s_r.at[p, 0], (ep, right)),
            remote(tt.at[far, p, half1], s1m.at[p], s_s.at[p, 1], s_r.at[p, 1], (ep, left)),
        )

    def d_copies(p):
        return (
            remote(tt.at[right, p, half1], dp.at[p], s_s.at[p, 2], s_r.at[p, 2], (ep, right)),
            remote(tt.at[left, p, half0], dm.at[p], s_s.at[p, 3], s_r.at[p, 3], (ep, left)),
        )

    def s2_copies(p):
        return (
            remote(sub_p.at[p], s2p.at[p], s_s.at[p, 4], s_r.at[p, 4], (ep, right)),
            remote(sub_m.at[p], s2m.at[p], s_s.at[p, 5], s_r.at[p, 5], (ep, left)),
        )

    def second(p):
        landed(s1_copies(p))
        sub_p[p] = (s1p[p].astype(F32) + tt[right, p, 0:256, :].astype(F32)).astype(BF)
        sub_m[p] = (s1m[p].astype(F32) + tt[left, p, 256:512, :].astype(F32)).astype(BF)
        begin(s2_copies(p))

    def total_of(p):
        landed(s2_copies(p))
        landed(d_copies(p))
        top = tt[t, p, 0:256, :].astype(F32) + s2p[p].astype(F32) + dm[p].astype(F32)
        low = tt[t, p, 256:512, :].astype(F32) + s2m[p].astype(F32) + dp[p].astype(F32)
        return top, low

    relay_step(0)
    relay_step(1)
    send_z(3)
    send_z(4)
    for c in wl:
        c.wait()
    routed(0)
    begin(x_copies(0))
    product(t, 0, first=True)
    relay_step(2)
    send_z(5)
    routed(1)
    begin(x_copies(1))
    product(t, 1)
    relay_step(3)
    forward_step(0)
    near_products(0)
    routed(2)
    begin(x_copies(2))
    product(t, 2)
    relay_step(4)
    forward_step(1)
    near_products(1)
    routed(3)
    begin(x_copies(3))
    product(t, 3)
    landed(f_copies(0))
    product(far, 0)

    seatcol = lax.broadcasted_iota(I32, (RELAY, 1), 0) // SEAT
    codes = zmeta[...].astype(F32)
    back0 = place(codes[:, 0:1], seatcol)
    back1 = place(codes[:, 1:2], seatcol)
    wide = lax.broadcasted_iota(I32, (RELAY, SLOTS), 1)
    m0 = jnp.where(wide == back0, 1.0, 0.0)
    m1 = jnp.where(wide == back1, 1.0, 0.0)
    c0[...] = m0.astype(BF)
    c1[...] = m1.astype(BF)
    c01[...] = (m0 + m1).astype(BF)

    relay_step(5)
    send_group(lambda r: scbuf.at[r], lambda r: scr.at[r], ys_s, ys_r)
    scr[mine, :] = scbuf[mine, :]
    landed(exch)
    forward_step(2)
    near_products(2)
    landed(f_copies(1))
    product(far, 1)
    routed(4)
    hb_part(0, True)
    forward_step(3)
    near_products(3)
    routed(5)
    hb_part(1, False)
    begin(s1_copies(4))
    begin(d_copies(4))
    landed(f_copies(2))
    product(far, 2)
    landed(f_copies(3))
    product(far, 3)

    drain(scbuf.at[most], ys_r)

    def hiddens(i, carry):
        at = pl.ds(pl.multiple_of(i * 64, 64), 64)
        gate, up = acc_gu[at, 0:128], acc_gu[at, 128:256]
        hid = gate * jax.nn.sigmoid(gate) * up
        wha[t, at, :] = (scr[at, :].astype(F32) * hid).astype(BF)
        return carry

    lax.fori_loop(0, 8, hiddens, 0)
    h_near = (
        remote(wha.at[t], wha.at[t], h_s.at[0], h_r.at[0], (ep, right)),
        remote(wha.at[t], wha.at[t], h_s.at[1], h_r.at[1], (ep, left)),
    )
    h_far = (
        remote(wha.at[left, half0], wha.at[left, half0], h_s.at[2], h_r.at[2], (ep, right)),
        remote(wha.at[right, half1], wha.at[right, half1], h_s.at[3], h_r.at[3], (ep, left)),
    )
    second(4)
    begin(h_near)
    hb_top, hb_low = total_of(4)
    acc_hb[0, 0:256, :] = hb_top
    acc_hb[0, 256:512, :] = hb_low

    def activate(i, carry):
        at = pl.ds(pl.multiple_of(i * 64, 64), 64)
        gate, up = acc_gu[at, 0:128], acc_gu[at, 128:256]
        hb = acc_hb[0, at, :]
        sc = scr[at, :].astype(F32)
        sig = jax.nn.sigmoid(gate)
        act = gate * sig
        hc = sc * hb
        cot[at, 0:128] = (hc * up * sig * (1.0 + gate * (1.0 - sig))).astype(BF)
        cot[at, 128:256] = (hc * act).astype(BF)
        rp[at, :] = act * up * hb
        return carry

    lax.fori_loop(0, 8, activate, 0)

    def share(k, p):
        at = pl.ds(pl.multiple_of(k * 512 + p * 256, 256), 256)
        part = mm(cot[...], wgu[at, :], NT).astype(BF)
        tt[k, 2 * p] = part[:, 0:128]
        tt[k, 2 * p + 1] = part[:, 128:256]

    def everyone(buf, ssem, rsem):
        return [
            remote(buf.at[t], buf.at[t], ssem.at[i], rsem.at[i], (ep, k))
            for i, k in enumerate((right, left, far))
        ]

    share(far, 0)
    begin(s1_copies(0))
    begin(s1_copies(1))
    share(right, 0)
    share(left, 0)
    begin(d_copies(0))
    ones16 = jnp.ones((16, 128), F32)
    rsum = mm(ones16, rp[...], NT, lax.Precision.HIGHEST)
    rall[t] = rsum[0:8, :]
    share(far, 1)
    share(right, 1)
    share(left, 1)
    r_copies = everyone(rall, r_s, r_r)
    begin(r_copies)
    share(t, 0)
    share(t, 1)

    def wgrad(j):
        k, h = j // 2, j % 2
        at = pl.ds(pl.multiple_of(j * 256, 256), 256)
        rows = jnp.concatenate([xs[k, 2 * h], xs[k, 2 * h + 1]], axis=1)
        both = mm(rows, cot[...], TN).astype(BF)
        ggb[at, :] = both[:, 0:128]
        gub[at, :] = both[:, 128:256]
        sq = jnp.square(both.astype(F32))
        ng = mm(ones16, sq[:, 0:128], NT, lax.Precision.HIGHEST)
        nu = mm(ones16, sq[:, 128:256], NT, lax.Precision.HIGHEST)
        rnall[t, pl.ds(2 * j, 1), :] = ng[0:1, 0:128]
        rnall[t, pl.ds(2 * j + 1, 1), :] = ng[0:1, 128:256]
        rnall[t, pl.ds(16 + 2 * j, 1), :] = nu[0:1, 0:128]
        rnall[t, pl.ds(17 + 2 * j, 1), :] = nu[0:1, 128:256]

    def wgrads(lo, hi):
        def body(j, carry):
            wgrad(j)
            return carry

        lax.fori_loop(lo, hi, body, 0)

    def reduced(p):
        top, low = total_of(p)
        ret[p, 0:256, :] = top.astype(BF)
        ret[p, 256:512, :] = low.astype(BF)
        send_group(lambda r: ret.at[p, r], lambda r: back.at[p, r], b_s.at[p], b_r.at[p])
        back[p, mine, :] = ret[p, mine, :]

    def home(src, dst, ssem, rsem):
        for d in (1, 2, 3):
            remote(src.at[pl.ds(d * SEAT, SEAT)], dst.at[seat(grp)], ssem, rsem, (in_z[d - 1], t)).start()

    def combine(p):
        drain(ret.at[p, most], b_r.at[p])
        tokbuf[p] = mm(c01[...], back[p]).astype(BF)
        home(tokbuf.at[p], srcv.at[p], zb_s.at[p], zb_r.at[p])
        srcv[p, seat(grp), :] = tokbuf[p, 0:SEAT, :]

    second(0)
    begin(d_copies(1))
    begin(s1_copies(2))
    wgrads(0, 2)
    second(1)
    begin(s1_copies(3))
    begin(d_copies(2))

    landed(r_copies)
    rtot = ((rall[0] + rall[1]) + rall[2]) + rall[3]
    rtot = jnp.where(lax.broadcasted_iota(I32, (8, SLOTS), 0) == 0, rtot, 0.0)
    retr[...] = mm(rtot.astype(BF), jnp.ones((8, 128), BF), TN).astype(BF)
    send_group(lambda r: retr.at[r], lambda r: backr.at[r], br_s, br_r)
    backr[mine, :] = retr[mine, :]

    landed(h_near)
    begin(h_far)
    reduced(0)
    second(2)
    begin(d_copies(3))
    wgrads(2, 4)
    reduced(1)
    second(3)
    wgrads(4, 6)

    landed(h_far)
    crows = [jnp.concatenate([cs[0], cs[1]], axis=1), jnp.concatenate([cs[2], cs[3]], axis=1)]

    def dgrad(k, carry):
        for c in range(2):
            gds[k, :, c * 256 : (c + 1) * 256] = mm(wha[k], crows[c], TN).astype(BF)
        return carry

    lax.fori_loop(0, 4, dgrad, 0)
    gdin[t] = gds[t]
    g_copies = [
        remote(gds.at[k], gdin.at[t], v_s.at[i], v_r.at[i], (ep, k))
        for i, k in enumerate((right, left, far))
    ]
    begin(g_copies)
    combine(0)
    reduced(2)
    combine(1)
    wgrads(6, 8)
    n_copies = everyone(rnall, n_s, n_r)
    begin(n_copies)
    reduced(3)
    drain(retr.at[most], br_r)
    lane2 = lax.broadcasted_iota(I32, (RELAY, 128), 1)
    rtb[...] = jnp.where(lane2 == 0, mm(c0[...], backr[...]), mm(c1[...], backr[...])).astype(BF)
    home(rtb, srcr, zr_s, zr_r)
    srcr[seat(grp), :] = rtb[0:SEAT, :]
    combine(2)

    landed(n_copies)
    norms = ((rnall[0] + rnall[1]) + rnall[2]) + rnall[3]
    gr_ref[...] = norms[0:16, :]
    ur_ref[...] = norms[16:32, :]
    landed(g_copies)
    total = jnp.zeros((128, 128), F32)
    for k in range(4):
        gdr[:, k * 512 : (k + 1) * 512] = gdin[k]
        sq = jnp.square(gdin[k].astype(F32))
        total += sq[:, 0:128] + sq[:, 128:256] + sq[:, 256:384] + sq[:, 384:512]
    dr_ref[...] = mm(ones16, total, NT, lax.Precision.HIGHEST)[0:1, :]
    combine(3)

    three = pl.ds(0, 3 * SEAT)
    drain(rtb.at[three], zr_r)
    rg_ref[...] = mm(srcr[...], t1[...], TN)[0:2, :].astype(BF)

    drain(sendmeta.at[three], zm_s)
    for i, (q0, n) in enumerate(CHUNKS):
        drain(sendbuf.at[pl.ds(q0, n), three], z_s.at[i])
        drain(pairbuf.at[pl.ds(q0, n), most], y_s.at[i])
    for i in range(4):
        left_here(x_copies(i))
        left_here(f_copies(i))
    drain(scbuf.at[most], ys_s)
    for group in (exch, h_near, h_far, r_copies, n_copies, g_copies):
        left_here(group)
    for p in range(5):
        left_here(s1_copies(p))
        left_here(d_copies(p))
        left_here(s2_copies(p))
    for p in range(4):
        drain(ret.at[p, most], b_s.at[p])
        drain(tokbuf.at[p, three], zb_s.at[p])
    drain(retr.at[most], br_s)
    drain(rtb.at[three], zr_s)
    for p in range(4):
        drain(tokbuf.at[p, three], zb_r.at[p])
        tg_ref[:, p * 128 : (p + 1) * 128] = mm(t1[...], srcv[p], TN).astype(BF)


def store(*refs):
    sems = refs[16]
    copies = [pltpu.make_async_copy(refs[i], refs[8 + i], sems.at[i]) for i in range(8)]
    for c in copies:
        c.start()
    for c in copies:
        c.wait()


def on_device(tokens, expert_ids, route_weights, cotangent, w_gate, w_up, w_down):
    vmem = pl.BlockSpec(memory_space=pltpu.VMEM)
    hbm = pl.BlockSpec(memory_space=pl.ANY)
    dma = pltpu.SemaphoreType.DMA
    v = pltpu.VMEM
    scratch = [
        v((TOK, 1024), BF),
        v((RELAY, TOK), BF),
        v((8, RELAY, 128), BF),
        v((RELAY, 128), BF),
        v((8, RELAY, 128), BF),
        v((RELAY, 128), BF),
        v((SLOTS, RELAY), BF),
        v((8, SLOTS, 128), BF),
        v((SLOTS, 128), BF),
        v((4, 4, SLOTS, 128), BF),
        v((4, SLOTS, 128), BF),
        v((SLOTS, 128), BF),
        v((2048, 256), BF),
        v((4, 128, 512), BF),
        v((SLOTS, 256), F32),
        v((4, SLOTS, 128), F32),
        v((SLOTS, 256), BF),
        v((4, SLOTS, 128), BF),
        v((SLOTS, 128), F32),
        v((4, 8, SLOTS), F32),
        v((4, 5, SLOTS, 128), BF),
        *[v((5, 256, 128), BF) for _ in range(8)],
        v((4, SLOTS, 128), BF),
        v((SLOTS, 128), BF),
        v((4, SLOTS, 128), BF),
        v((SLOTS, 128), BF),
        v((RELAY, SLOTS), BF),
        v((RELAY, SLOTS), BF),
        v((RELAY, SLOTS), BF),
        v((4, RELAY, 128), BF),
        v((RELAY, 128), BF),
        v((4, RELAY, 128), BF),
        v((RELAY, 128), BF),
        v((4, 128, 512), BF),
        v((4, 128, 512), BF),
        v((4, 32, 128), F32),
        v((2, TOK), I32),
        v((2, TOK), BF),
        dma((4,)), dma((3,)),
        dma((6,)), dma((6,)), dma(()), dma(()),
        dma((6,)), dma((6,)), dma(()), dma(()),
        dma((4, 4)), dma((4, 4)),
        dma((4,)), dma((4,)),
        dma((3,)), dma((3,)),
        dma((3,)), dma((3,)),
        dma((3,)), dma((3,)),
        dma((5, 6)), dma((5, 6)),
        dma((4,)), dma((4,)), dma(()), dma(()),
        dma((4,)), dma((4,)), dma(()), dma(()),
        dma((3,)), dma((3,)),
    ]
    outs = (
        v((TOK, 512), BF), v((2, TOK), BF), v((2048, 128), BF), v((2048, 128), BF),
        v((128, 2048), BF), v((16, 128), F32), v((16, 128), F32), v((1, 128), F32),
    )
    held = pl.pallas_call(
        kernel,
        out_shape=outs,
        in_specs=[hbm] * 7,
        out_specs=(vmem,) * 8,
        scratch_shapes=scratch,
        compiler_params=pltpu.CompilerParams(collective_id=0, has_side_effects=True),
    )(expert_ids.T, route_weights.T, tokens, cotangent, w_gate[0], w_up[0], w_down[0])
    tg, rg, gg, gu, gd, gr, ur, dr = pl.pallas_call(
        store,
        out_shape=tuple(jax.ShapeDtypeStruct(o.shape, o.dtype) for o in outs),
        in_specs=[vmem] * 8,
        out_specs=(hbm,) * 8,
        scratch_shapes=[dma((8,))],
    )(*[pltpu.with_memory_space_constraint(h, pltpu.VMEM) for h in held])
    return (
        tg, rg.T, gg[None], gu[None], gd[None],
        gr.reshape(1, 2048), ur.reshape(1, 2048), dr,
    )


def solution(mesh):
    return jax.shard_map(
        on_device,
        mesh=mesh,
        in_specs=(
            P("ep", None), P("ep", None), P("ep", None), P("ep", None),
            P("ep", None, "tp"), P("ep", None, "tp"), P("ep", "tp", None),
        ),
        out_specs=(
            P("ep", "tp"), P("ep", None), P("ep", None, "tp"), P("ep", None, "tp"),
            P("ep", "tp", None), P("ep", None), P("ep", None), P("ep", "tp"),
        ),
        check_vma=False,
    )
```

time: 122 us -> 99.5 us (0.82)
  Pallas kernels: 113 us -> 98.7 us
  local copies, waits for them, and re-layouts: 7.93 us -> 0 us
    pallas_call x1 -> x2, Pallas kernels: 113 us -> 98.7 us  [the longest x1 97.5 us: on_device(): pl.pallas_call(kernel, out_shape=outs, in_specs=[hbm] * 7, out_specs=(vme...]
    unnamed x20 -> x0, local copies, waits for them, and re-layouts: 7.93 us -> none
where the time goes in v2:
time: 99.5 us; the launch traced here: 99.4 us
  Pallas kernels  98.7 us (99%)
    pallas_call x1, Pallas kernels, on_device(): pl.pallas_call(kernel, out_shape=outs, in_specs=[hbm] * 7, out_specs=(vme...  97.5 us

profile of v2, /device:TPU:1, one launch (start us, length us, event | category | flops | bytes accessed | tf_op | source)
XLA Modules:
  0.0 99.4 jit_solution(4070746777808311373)
XLA Ops:
  0.6 97.5 %shard_map.134 = (bf16[128,512]{1,0:T(8,128)(2,1)S(1)}, bf16[2,128]{1,0:T(2,128)(2,1)S(1)}, bf16[2048,128]{1,0:T(8,128)(2,1)S(1)}, bf16[2048,128]{1,0:T(8,128)(2...) custom-call(s32[2,128]{1,0:T(2,128)} %bitcast.14, ...), custom_call_target="tpu_custom_call" | custom-call | tf_op jit(solution)/shard_map/pallas_call | solution.py:666
  98.1 1.3 %shard_map.135 = (bf16[128,512]{1,0:T(8,128)(2,1)}, bf16[2,128]{1,0:T(2,128)(2,1)}, bf16[2048,128]{1,0:T(8,128)(2,1)}, bf16[2048,128]{1,0:T(8,128)(2,1)}, bf16[1...) custom-call(bf16[128,512]{1,0:T(8,128)(2,1)S(1)} %get-tuple-element.24.refs_0_, ...), custom_call_target="tpu_custom_call" | custom-call | tf_op jit(solution)/shard_map/pallas_call | solution.py:674

commit v3 on v2

--- a/solution.py
+++ b/solution.py
@@ -33,11 +33,10 @@
 def kernel(
     ids_hbm, rw_hbm, tok_hbm, cot_hbm, wg_hbm, wu_hbm, wd_hbm,
     tg_ref, rg_ref, ggb, gub, gdr, gr_ref, ur_ref, dr_ref,
-    xc, t1, sendbuf, sendmeta, relay, zmeta, p2, pairbuf, scbuf, xs, cs, scr,
-    wgu, wdd, acc_gu, acc_hb, cot, wha, rp, rall, tt, sub_p, sub_m,
-    s1p, s1m, dp, dm, s2p, s2m, ret, retr, back, backr, c01, c0, c1,
+    xc, t1, sendbuf, sendmeta, relay, zmeta, p2, pairbuf, scbuf, scin, xs, cs, scr,
+    wgu, wdd, wp, wq, acc_gu, acc_hb, hbp, hbr, cot, cotp, cotq, wha, rp, rall, ts, rsv, own, ret, retr, back, backr, c01, c0, c1,
     tokbuf, rtb, srcv, srcr, gds, gdin, rnall, ids_v, rw_v,
-    ld_s, w_s, z_s, z_r, zm_s, zm_r, y_s, y_r, ys_s, ys_r, x_s, x_r, h_s, h_r, v_s, v_r, e_s, e_r,
+    ld_s, w_s, z_s, z_r, zm_s, zm_r, y_s, y_r, ys_s, ys_r, x_s, x_r, h_s, h_r, v_s, v_r, e_s, e_r, u_s, u_r, k_s, k_r, c_s, c_r,
     r_s, r_r, s_s, s_r, b_s, b_r, br_s, br_r, zb_s, zb_r, zr_s, zr_r, n_s, n_r,
 ):
     ep = lax.axis_index("ep")
@@ -51,6 +50,8 @@
     right = (t + 1) % 4
     left = (t + 3) % 4
     far = (t + 2) % 4
+    one = t + 1 - 2 * (t % 2)
+    two = 3 - t
 
     def plane(off):
         return ((z + off + PLANES) % PLANES) * ROW + yc
@@ -91,6 +92,14 @@
     def block(k):
         return pl.ds(pl.multiple_of(k * 512, 512), 512)
 
+    barrier = pltpu.get_barrier_semaphore()
+
+    def hello(e, k):
+        pl.semaphore_signal(barrier, inc=1, device_id=(e, k), device_id_type=MESH)
+
+    for e in (plane(-3 * sg), plane(2), plane(-2), plane(-sg)):
+        hello(e, t)
+
     route_in = [
         pltpu.make_async_copy(ids_hbm, ids_v, ld_s.at[2]),
         pltpu.make_async_copy(rw_hbm, rw_v, ld_s.at[3]),
@@ -107,13 +116,6 @@
     ]
     begin(ld)
 
-    barrier = pltpu.get_barrier_semaphore()
-
-    def hello(e, k):
-        pl.semaphore_signal(barrier, inc=1, device_id=(e, k), device_id_type=MESH)
-
-    for e in (plane(-3 * sg), plane(2), plane(-2), plane(-sg)):
-        hello(e, t)
     for k in (far, right, left):
         hello(ep, k)
 
@@ -184,6 +186,15 @@
     zmeta[0:SEAT, :] = sendmeta[seat(grp), :]
     for h in range(8):
         relay[h, 0:SEAT, :] = sendbuf[h, seat(grp), :]
+    for c in wl:
+        c.wait()
+    swap = [
+        remote(wgu.at[block(two)], wq.at[0], u_s.at[0], u_r.at[0], (ep, two)),
+        remote(wgu.at[block(one)], wp.at[0], u_s.at[1], u_r.at[1], (ep, one)),
+        remote(wgu.at[block(far)], wq.at[1], u_s.at[2], u_r.at[2], (ep, two)),
+        remote(wgu.at[block(far)], wp.at[1], u_s.at[3], u_r.at[3], (ep, one)),
+    ]
+    begin(swap)
 
     drain(zmeta.at[pl.ds(SEAT, 3 * SEAT)], zm_r)
     send_z(2)
@@ -199,16 +210,12 @@
 
     pos0 = place(flat[0:1, :], seatrow)
     pos1 = place(flat[1:2, :], seatrow)
-    w0, w1 = flat[2:3, :], flat[3:4, :]
-    ones256 = jnp.ones((RELAY, 128), BF)
 
     def spread(i, carry):
         at = pl.ds(pl.multiple_of(i * 128, 128), 128)
         p = lax.broadcasted_iota(I32, (128, RELAY), 0) + i * 128
         e0, e1 = p == pos0, p == pos1
         p2[at, :] = jnp.where(e0, 1.0, jnp.where(e1, 1.0, 0.0)).astype(BF)
-        weights = (jnp.where(e0, w0, 0.0) + jnp.where(e1, w1, 0.0)).astype(BF)
-        scbuf[at, :] = mm(weights, ones256).astype(BF)
         return carry
 
     lax.fori_loop(0, 4, spread, 0)
@@ -294,73 +301,59 @@
             if first:
                 acc_hb[k] = part
             else:
-                tt[k, 4] = (acc_hb[k] + part).astype(BF)
+                whole = acc_hb[k] + part
+                acc_hb[k] = whole
+                hbp[k] = whole.astype(BF)
             return carry
 
         lax.fori_loop(0, 4, body, 0)
-
-    def s1_copies(p):
-        return (
-            remote(tt.at[far, p, half0], s1p.at[p], s_s.at[p, 0], s_r.at[p, 0], (ep, right)),
-            remote(tt.at[far, p, half1], s1m.at[p], s_s.at[p, 1], s_r.at[p, 1], (ep, left)),
-        )
-
-    def d_copies(p):
-        return (
-            remote(tt.at[right, p, half1], dp.at[p], s_s.at[p, 2], s_r.at[p, 2], (ep, right)),
-            remote(tt.at[left, p, half0], dm.at[p], s_s.at[p, 3], s_r.at[p, 3], (ep, left)),
-        )
-
-    def s2_copies(p):
-        return (
-            remote(sub_p.at[p], s2p.at[p], s_s.at[p, 4], s_r.at[p, 4], (ep, right)),
-            remote(sub_m.at[p], s2m.at[p], s_s.at[p, 5], s_r.at[p, 5], (ep, left)),
-        )
-
-    def second(p):
-        landed(s1_copies(p))
-        sub_p[p] = (s1p[p].astype(F32) + tt[right, p, 0:256, :].astype(F32)).astype(BF)
-        sub_m[p] = (s1m[p].astype(F32) + tt[left, p, 256:512, :].astype(F32)).astype(BF)
-        begin(s2_copies(p))
-
-    def total_of(p):
-        landed(s2_copies(p))
-        landed(d_copies(p))
-        top = tt[t, p, 0:256, :].astype(F32) + s2p[p].astype(F32) + dm[p].astype(F32)
-        low = tt[t, p, 256:512, :].astype(F32) + s2m[p].astype(F32) + dp[p].astype(F32)
-        return top, low
 
     relay_step(0)
     relay_step(1)
     send_z(3)
     send_z(4)
-    for c in wl:
-        c.wait()
     routed(0)
     begin(x_copies(0))
     product(t, 0, first=True)
     relay_step(2)
     send_z(5)
+
+    seatcol = lax.broadcasted_iota(I32, (RELAY, 1), 0) // SEAT
+    codes = zmeta[...].astype(F32)
+    lanes = lax.broadcasted_iota(I32, (RELAY, 128), 1)
+
+    def weight_rows(k):
+        code = codes[:, k : k + 1].astype(I32)
+        to = jnp.where(lanes == code // 4, 1.0, 0.0).astype(BF)
+        at = jnp.where(lanes == seatcol * 4 + code % 4, codes[:, k + 2 : k + 3], 0.0).astype(BF)
+        return mm(to, at, TN)
+
+    table = weight_rows(0) + weight_rows(1)
+    for e in range(GROUP):
+        scbuf[e] = table[e : e + 1, :]
+
+    def send_weights(o, carry):
+        e = peer(o)
+        remote(scbuf.at[e], scin.at[loc], ys_s, ys_r, (base + e, t)).start()
+        return carry
+
+    lax.fori_loop(1, GROUP, send_weights, 0)
+    scin[loc] = scbuf[loc]
     routed(1)
     begin(x_copies(1))
     product(t, 1)
     relay_step(3)
-    forward_step(0)
-    near_products(0)
+    relay_step(4)
     routed(2)
     begin(x_copies(2))
     product(t, 2)
-    relay_step(4)
-    forward_step(1)
-    near_products(1)
+    forward_step(0)
+    near_products(0)
     routed(3)
     begin(x_copies(3))
     product(t, 3)
-    landed(f_copies(0))
-    product(far, 0)
-
-    seatcol = lax.broadcasted_iota(I32, (RELAY, 1), 0) // SEAT
-    codes = zmeta[...].astype(F32)
+    relay_step(5)
+
     back0 = place(codes[:, 0:1], seatcol)
     back1 = place(codes[:, 1:2], seatcol)
     wide = lax.broadcasted_iota(I32, (RELAY, SLOTS), 1)
@@ -370,56 +363,51 @@
     c1[...] = m1.astype(BF)
     c01[...] = (m0 + m1).astype(BF)
 
-    relay_step(5)
-    send_group(lambda r: scbuf.at[r], lambda r: scr.at[r], ys_s, ys_r)
-    scr[mine, :] = scbuf[mine, :]
+    forward_step(1)
+    near_products(1)
     landed(exch)
     forward_step(2)
     near_products(2)
-    landed(f_copies(1))
-    product(far, 1)
     routed(4)
     hb_part(0, True)
+    landed(f_copies(0))
+    product(far, 0)
     forward_step(3)
-    near_products(3)
     routed(5)
     hb_part(1, False)
-    begin(s1_copies(4))
-    begin(d_copies(4))
-    landed(f_copies(2))
-    product(far, 2)
-    landed(f_copies(3))
-    product(far, 3)
-
-    drain(scbuf.at[most], ys_r)
+    k_copies = [
+        remote(hbp.at[k], hbr.at[i], k_s.at[i], k_r.at[i], (ep, k))
+        for i, k in enumerate((far, right, left))
+    ]
+    begin(k_copies)
+    near_products(3)
+    for i in (1, 2, 3):
+        landed(f_copies(i))
+        product(far, i)
+
+    drain(scbuf.at[pl.ds(0, GROUP - 1)], ys_r)
+    prow = lax.broadcasted_iota(I32, (SLOTS, GROUP), 0)
+    from_relay = jnp.where(prow // BLK == lax.broadcasted_iota(I32, (SLOTS, GROUP), 1), 1.0, 0.0)
+    listed = mm(from_relay.astype(BF), scin[:, 0, :].astype(BF))
+    inside = lax.broadcasted_iota(I32, (SLOTS, 128), 0) % BLK == lax.broadcasted_iota(I32, (SLOTS, 128), 1)
+    scr[...] = mm(jnp.where(inside, listed, 0.0).astype(BF), jnp.ones((128, 128), BF))
 
     def hiddens(i, carry):
         at = pl.ds(pl.multiple_of(i * 64, 64), 64)
         gate, up = acc_gu[at, 0:128], acc_gu[at, 128:256]
         hid = gate * jax.nn.sigmoid(gate) * up
-        wha[t, at, :] = (scr[at, :].astype(F32) * hid).astype(BF)
+        wha[t, at, :] = (scr[at, :] * hid).astype(BF)
         return carry
 
     lax.fori_loop(0, 8, hiddens, 0)
-    h_near = (
-        remote(wha.at[t], wha.at[t], h_s.at[0], h_r.at[0], (ep, right)),
-        remote(wha.at[t], wha.at[t], h_s.at[1], h_r.at[1], (ep, left)),
-    )
-    h_far = (
-        remote(wha.at[left, half0], wha.at[left, half0], h_s.at[2], h_r.at[2], (ep, right)),
-        remote(wha.at[right, half1], wha.at[right, half1], h_s.at[3], h_r.at[3], (ep, left)),
-    )
-    second(4)
-    begin(h_near)
-    hb_top, hb_low = total_of(4)
-    acc_hb[0, 0:256, :] = hb_top
-    acc_hb[0, 256:512, :] = hb_low
+    landed(k_copies)
 
     def activate(i, carry):
         at = pl.ds(pl.multiple_of(i * 64, 64), 64)
         gate, up = acc_gu[at, 0:128], acc_gu[at, 128:256]
-        hb = acc_hb[0, at, :]
-        sc = scr[at, :].astype(F32)
+        hb = acc_hb[t, at, :] + hbr[0, at, :].astype(F32)
+        hb = hb + hbr[1, at, :].astype(F32) + hbr[2, at, :].astype(F32)
+        sc = scr[at, :]
         sig = jax.nn.sigmoid(gate)
         act = gate * sig
         hc = sc * hb
@@ -430,34 +418,45 @@
 
     lax.fori_loop(0, 8, activate, 0)
 
-    def share(k, p):
-        at = pl.ds(pl.multiple_of(k * 512 + p * 256, 256), 256)
-        part = mm(cot[...], wgu[at, :], NT).astype(BF)
-        tt[k, 2 * p] = part[:, 0:128]
-        tt[k, 2 * p + 1] = part[:, 128:256]
-
     def everyone(buf, ssem, rsem):
         return [
             remote(buf.at[t], buf.at[t], ssem.at[i], rsem.at[i], (ep, k))
             for i, k in enumerate((right, left, far))
         ]
 
-    share(far, 0)
-    begin(s1_copies(0))
-    begin(s1_copies(1))
-    share(right, 0)
-    share(left, 0)
-    begin(d_copies(0))
+    c_copies = [
+        remote(cot.at[half0], cotp, c_s.at[0], c_r.at[0], (ep, one)),
+        remote(cot.at[half1], cotq, c_s.at[1], c_r.at[1], (ep, two)),
+    ]
+    begin(c_copies)
     ones16 = jnp.ones((16, 128), F32)
     rsum = mm(ones16, rp[...], NT, lax.Precision.HIGHEST)
     rall[t] = rsum[0:8, :]
-    share(far, 1)
-    share(right, 1)
-    share(left, 1)
-    r_copies = everyone(rall, r_s, r_r)
-    begin(r_copies)
-    share(t, 0)
-    share(t, 1)
+
+    def partial(rows, mine_at, near, near_w, p):
+        at = pl.ds(pl.multiple_of(mine_at * 512 + p * 256, 256), 256)
+        part = mm(cot[rows], wgu[at, :], NT)
+        return part + mm(near[...], near_w[p * 256 : (p + 1) * 256, :], NT)
+
+    def away(p):
+        top = partial(slice(0, 256), two, cotp, wp[1], p).astype(BF)
+        low = partial(slice(256, 512), one, cotq, wq[1], p).astype(BF)
+        for k in range(2):
+            ts[0, 2 * p + k] = top[:, k * 128 : (k + 1) * 128]
+            ts[1, 2 * p + k] = low[:, k * 128 : (k + 1) * 128]
+
+    def kept(p):
+        top = partial(slice(0, 256), t, cotp, wp[0], p)
+        low = partial(slice(256, 512), t, cotq, wq[0], p)
+        for k in range(2):
+            own[2 * p + k, 0:256, :] = top[:, k * 128 : (k + 1) * 128]
+            own[2 * p + k, 256:512, :] = low[:, k * 128 : (k + 1) * 128]
+
+    def t_copies(p):
+        return (
+            remote(ts.at[0, p], rsv.at[0, p], s_s.at[p, 0], s_r.at[p, 0], (ep, two)),
+            remote(ts.at[1, p], rsv.at[1, p], s_s.at[p, 1], s_r.at[p, 1], (ep, one)),
+        )
 
     def wgrad(j):
         k, h = j // 2, j % 2
@@ -482,9 +481,9 @@
         lax.fori_loop(lo, hi, body, 0)
 
     def reduced(p):
-        top, low = total_of(p)
-        ret[p, 0:256, :] = top.astype(BF)
-        ret[p, 256:512, :] = low.astype(BF)
+        landed(t_copies(p))
+        ret[p, 0:256, :] = (own[p, 0:256, :] + rsv[0, p].astype(F32)).astype(BF)
+        ret[p, 256:512, :] = (own[p, 256:512, :] + rsv[1, p].astype(F32)).astype(BF)
         send_group(lambda r: ret.at[p, r], lambda r: back.at[p, r], b_s.at[p], b_r.at[p])
         back[p, mine, :] = ret[p, mine, :]
 
@@ -498,30 +497,40 @@
         home(tokbuf.at[p], srcv.at[p], zb_s.at[p], zb_r.at[p])
         srcv[p, seat(grp), :] = tokbuf[p, 0:SEAT, :]
 
-    second(0)
-    begin(d_copies(1))
-    begin(s1_copies(2))
+    r_copies = everyone(rall, r_s, r_r)
+    begin(r_copies)
     wgrads(0, 2)
-    second(1)
-    begin(s1_copies(3))
-    begin(d_copies(2))
+    h_near = (
+        remote(wha.at[t], wha.at[t], h_s.at[0], h_r.at[0], (ep, right)),
+        remote(wha.at[t], wha.at[t], h_s.at[1], h_r.at[1], (ep, left)),
+    )
+    h_far = (
+        remote(wha.at[left, half0], wha.at[left, half0], h_s.at[2], h_r.at[2], (ep, right)),
+        remote(wha.at[right, half1], wha.at[right, half1], h_s.at[3], h_r.at[3], (ep, left)),
+    )
+    begin(h_near)
+    landed(swap)
+    landed(c_copies)
+    away(0)
+    begin(t_copies(0))
+    away(1)
 
     landed(r_copies)
     rtot = ((rall[0] + rall[1]) + rall[2]) + rall[3]
     rtot = jnp.where(lax.broadcasted_iota(I32, (8, SLOTS), 0) == 0, rtot, 0.0)
     retr[...] = mm(rtot.astype(BF), jnp.ones((8, 128), BF), TN).astype(BF)
+    begin(t_copies(1))
     send_group(lambda r: retr.at[r], lambda r: backr.at[r], br_s, br_r)
     backr[mine, :] = retr[mine, :]
-
+    kept(0)
+    begin(t_copies(2))
     landed(h_near)
     begin(h_far)
     reduced(0)
-    second(2)
-    begin(d_copies(3))
-    wgrads(2, 4)
+    begin(t_copies(3))
+    kept(1)
+    wgrads(2, 3)
     reduced(1)
-    second(3)
-    wgrads(4, 6)
 
     landed(h_far)
     crows = [jnp.concatenate([cs[0], cs[1]], axis=1), jnp.concatenate([cs[2], cs[3]], axis=1)]
@@ -535,27 +544,28 @@
     gdin[t] = gds[t]
     g_copies = [
         remote(gds.at[k], gdin.at[t], v_s.at[i], v_r.at[i], (ep, k))
-        for i, k in enumerate((right, left, far))
+        for i, k in enumerate((far, right, left))
     ]
     begin(g_copies)
+    reduced(2)
+    wgrads(3, 5)
+    reduced(3)
     combine(0)
-    reduced(2)
-    combine(1)
-    wgrads(6, 8)
+    wgrads(5, 8)
     n_copies = everyone(rnall, n_s, n_r)
     begin(n_copies)
-    reduced(3)
+    combine(1)
     drain(retr.at[most], br_r)
     lane2 = lax.broadcasted_iota(I32, (RELAY, 128), 1)
     rtb[...] = jnp.where(lane2 == 0, mm(c0[...], backr[...]), mm(c1[...], backr[...])).astype(BF)
     home(rtb, srcr, zr_s, zr_r)
     srcr[seat(grp), :] = rtb[0:SEAT, :]
-    combine(2)
-
     landed(n_copies)
     norms = ((rnall[0] + rnall[1]) + rnall[2]) + rnall[3]
     gr_ref[...] = norms[0:16, :]
     ur_ref[...] = norms[16:32, :]
+    combine(2)
+    combine(3)
     landed(g_copies)
     total = jnp.zeros((128, 128), F32)
     for k in range(4):
@@ -563,7 +573,6 @@
         sq = jnp.square(gdin[k].astype(F32))
         total += sq[:, 0:128] + sq[:, 128:256] + sq[:, 256:384] + sq[:, 384:512]
     dr_ref[...] = mm(ones16, total, NT, lax.Precision.HIGHEST)[0:1, :]
-    combine(3)
 
     three = pl.ds(0, 3 * SEAT)
     drain(rtb.at[three], zr_r)
@@ -576,14 +585,11 @@
     for i in range(4):
         left_here(x_copies(i))
         left_here(f_copies(i))
-    drain(scbuf.at[most], ys_s)
-    for group in (exch, h_near, h_far, r_copies, n_copies, g_copies):
+    drain(scbuf.at[pl.ds(0, GROUP - 1)], ys_s)
+    for group in (exch, swap, k_copies, c_copies, h_near, h_far, r_copies, n_copies, g_copies):
         left_here(group)
-    for p in range(5):
-        left_here(s1_copies(p))
-        left_here(d_copies(p))
-        left_here(s2_copies(p))
     for p in range(4):
+        left_here(t_copies(p))
         drain(ret.at[p, most], b_s.at[p])
         drain(tokbuf.at[p, three], zb_s.at[p])
     drain(retr.at[most], br_s)
@@ -616,20 +622,28 @@
         v((RELAY, 128), BF),
         v((SLOTS, RELAY), BF),
         v((8, SLOTS, 128), BF),
-        v((SLOTS, 128), BF),
+        v((GROUP, 1, 128), F32),
+        v((GROUP, 1, 128), F32),
         v((4, 4, SLOTS, 128), BF),
         v((4, SLOTS, 128), BF),
-        v((SLOTS, 128), BF),
+        v((SLOTS, 128), F32),
         v((2048, 256), BF),
         v((4, 128, 512), BF),
+        v((2, 512, 256), BF),
+        v((2, 512, 256), BF),
         v((SLOTS, 256), F32),
         v((4, SLOTS, 128), F32),
+        v((4, SLOTS, 128), BF),
+        v((3, SLOTS, 128), BF),
         v((SLOTS, 256), BF),
+        v((256, 256), BF),
+        v((256, 256), BF),
         v((4, SLOTS, 128), BF),
         v((SLOTS, 128), F32),
         v((4, 8, SLOTS), F32),
-        v((4, 5, SLOTS, 128), BF),
-        *[v((5, 256, 128), BF) for _ in range(8)],
+        v((2, 4, 256, 128), BF),
+        v((2, 4, 256, 128), BF),
+        v((4, SLOTS, 128), F32),
         v((4, SLOTS, 128), BF),
         v((SLOTS, 128), BF),
         v((4, SLOTS, 128), BF),
@@ -653,8 +667,11 @@
         dma((4,)), dma((4,)),
         dma((3,)), dma((3,)),
         dma((3,)), dma((3,)),
+        dma((4,)), dma((4,)),
         dma((3,)), dma((3,)),
-        dma((5, 6)), dma((5, 6)),
+        dma((2,)), dma((2,)),
+        dma((3,)), dma((3,)),
+        dma((4, 2)), dma((4, 2)),
         dma((4,)), dma((4,)), dma(()), dma(()),
         dma((4,)), dma((4,)), dma(()), dma(()),
         dma((3,)), dma((3,)),

time: 99.5 us -> 92.1 us (0.926)
  Pallas kernels: 98.7 us -> 91.3 us
    pallas_call x1, Pallas kernels: 97.5 us -> 90 us  [on_device(): pl.pallas_call(kernel, out_shape=outs, in_specs=[hbm] * 7, out_specs=(vme...]
where the time goes in v3:
time: 92.1 us; the launch traced here: 91.9 us
  Pallas kernels  91.3 us (99%)
    pallas_call x1, Pallas kernels, on_device(): pl.pallas_call(kernel, out_shape=outs, in_specs=[hbm] * 7, out_specs=(vme...  90 us

profile of v3, /device:TPU:1, one launch (start us, length us, event | category | flops | bytes accessed | tf_op | source)
XLA Modules:
  0.0 91.9 jit_solution(10848860097251741614)
XLA Ops:
  0.6 90.0 %shard_map.134 = (bf16[128,512]{1,0:T(8,128)(2,1)S(1)}, bf16[2,128]{1,0:T(2,128)(2,1)S(1)}, bf16[2048,128]{1,0:T(8,128)(2,1)S(1)}, bf16[2048,128]{1,0:T(8,128)(2...) custom-call(s32[2,128]{1,0:T(2,128)} %bitcast.14, ...), custom_call_target="tpu_custom_call" | custom-call | tf_op jit(solution)/shard_map/pallas_call | solution.py:683
  90.6 1.3 %shard_map.135 = (bf16[128,512]{1,0:T(8,128)(2,1)}, bf16[2,128]{1,0:T(2,128)(2,1)}, bf16[2048,128]{1,0:T(8,128)(2,1)}, bf16[2048,128]{1,0:T(8,128)(2,1)}, bf16[1...) custom-call(bf16[128,512]{1,0:T(8,128)(2,1)S(1)} %get-tuple-element.24.refs_0_, ...), custom_call_target="tpu_custom_call" | custom-call | tf_op jit(solution)/shard_map/pallas_call | solution.py:691

commit v4 on v3

--- a/solution.py
+++ b/solution.py
@@ -293,20 +293,20 @@
 
         lax.fori_loop(0, 2, body, 0)
 
-    def hb_part(c, first):
-        rows = jnp.concatenate([cs[2 * c], cs[2 * c + 1]], axis=1)
+    def hb_rows(c):
+        return jnp.concatenate([cs[2 * c], cs[2 * c + 1]], axis=1)
+
+    def hb_start():
+        rows = hb_rows(0)
 
         def body(k, carry):
-            part = mm(rows, wdd[k, :, c * 256 : (c + 1) * 256], NT)
-            if first:
-                acc_hb[k] = part
-            else:
-                whole = acc_hb[k] + part
-                acc_hb[k] = whole
-                hbp[k] = whole.astype(BF)
+            acc_hb[k] = mm(rows, wdd[k, :, 0:256], NT)
             return carry
 
         lax.fori_loop(0, 4, body, 0)
+
+    def hb_whole(k):
+        return acc_hb[k] + mm(hb_rows(1), wdd[k, :, 256:512], NT)
 
     relay_step(0)
     relay_step(1)
@@ -348,11 +348,11 @@
     begin(x_copies(2))
     product(t, 2)
     forward_step(0)
+    relay_step(5)
     near_products(0)
     routed(3)
     begin(x_copies(3))
     product(t, 3)
-    relay_step(5)
 
     back0 = place(codes[:, 0:1], seatcol)
     back1 = place(codes[:, 1:2], seatcol)
@@ -369,17 +369,19 @@
     forward_step(2)
     near_products(2)
     routed(4)
-    hb_part(0, True)
+    hb_start()
     landed(f_copies(0))
     product(far, 0)
     forward_step(3)
     routed(5)
-    hb_part(1, False)
     k_copies = [
         remote(hbp.at[k], hbr.at[i], k_s.at[i], k_r.at[i], (ep, k))
         for i, k in enumerate((far, right, left))
     ]
-    begin(k_copies)
+    for i, k in enumerate((far, right, left)):
+        hbp[k] = hb_whole(k).astype(BF)
+        k_copies[i].start()
+    acc_hb[t] = hb_whole(t)
     near_products(3)
     for i in (1, 2, 3):
         landed(f_copies(i))
@@ -416,7 +418,7 @@
         rp[at, :] = act * up * hb
         return carry
 
-    lax.fori_loop(0, 8, activate, 0)
+    lax.fori_loop(0, 4, activate, 0)
 
     def everyone(buf, ssem, rsem):
         return [
@@ -428,7 +430,9 @@
         remote(cot.at[half0], cotp, c_s.at[0], c_r.at[0], (ep, one)),
         remote(cot.at[half1], cotq, c_s.at[1], c_r.at[1], (ep, two)),
     ]
-    begin(c_copies)
+    c_copies[0].start()
+    lax.fori_loop(4, 8, activate, 0)
+    c_copies[1].start()
     ones16 = jnp.ones((16, 128), F32)
     rsum = mm(ones16, rp[...], NT, lax.Precision.HIGHEST)
     rall[t] = rsum[0:8, :]
@@ -499,7 +503,7 @@
 
     r_copies = everyone(rall, r_s, r_r)
     begin(r_copies)
-    wgrads(0, 2)
+    wgrads(0, 3)
     h_near = (
         remote(wha.at[t], wha.at[t], h_s.at[0], h_r.at[0], (ep, right)),
         remote(wha.at[t], wha.at[t], h_s.at[1], h_r.at[1], (ep, left)),
@@ -529,7 +533,6 @@
     reduced(0)
     begin(t_copies(3))
     kept(1)
-    wgrads(2, 3)
     reduced(1)
 
     landed(h_far)
@@ -575,6 +578,13 @@
     dr_ref[...] = mm(ones16, total, NT, lax.Precision.HIGHEST)[0:1, :]
 
     three = pl.ds(0, 3 * SEAT)
+
+    def finish(p):
+        drain(tokbuf.at[p, three], zb_r.at[p])
+        tg_ref[:, p * 128 : (p + 1) * 128] = mm(t1[...], srcv[p], TN).astype(BF)
+
+    finish(0)
+    finish(1)
     drain(rtb.at[three], zr_r)
     rg_ref[...] = mm(srcr[...], t1[...], TN)[0:2, :].astype(BF)
 
@@ -594,9 +604,8 @@
         drain(tokbuf.at[p, three], zb_s.at[p])
     drain(retr.at[most], br_s)
     drain(rtb.at[three], zr_s)
-    for p in range(4):
-        drain(tokbuf.at[p, three], zb_r.at[p])
-        tg_ref[:, p * 128 : (p + 1) * 128] = mm(t1[...], srcv[p], TN).astype(BF)
+    finish(2)
+    finish(3)
 
 
 def store(*refs):

time: 92.1 us -> 90.8 us (0.986)
  Pallas kernels: 91.3 us -> 89.5 us
    pallas_call x1, Pallas kernels: 90 us -> 88.2 us  [on_device(): pl.pallas_call(kernel, out_shape=outs, in_specs=[hbm] * 7, out_specs=(vme...]
where the time goes in v4:
time: 90.8 us; the launch traced here: 90.1 us
  Pallas kernels  89.5 us (99%)
    pallas_call x1, Pallas kernels, on_device(): pl.pallas_call(kernel, out_shape=outs, in_specs=[hbm] * 7, out_specs=(vme...  88.2 us

profile of v4, /device:TPU:1, one launch (start us, length us, event | category | flops | bytes accessed | tf_op | source)
XLA Modules:
  0.0 90.1 jit_solution(16260705755238570531)
XLA Ops:
  0.6 88.2 %shard_map.134 = (bf16[128,512]{1,0:T(8,128)(2,1)S(1)}, bf16[2,128]{1,0:T(2,128)(2,1)S(1)}, bf16[2048,128]{1,0:T(8,128)(2,1)S(1)}, bf16[2048,128]{1,0:T(8,128)(2...) custom-call(s32[2,128]{1,0:T(2,128)} %bitcast.14, ...), custom_call_target="tpu_custom_call" | custom-call | tf_op jit(solution)/shard_map/pallas_call | solution.py:692
  88.8 1.3 %shard_map.135 = (bf16[128,512]{1,0:T(8,128)(2,1)}, bf16[2,128]{1,0:T(2,128)(2,1)}, bf16[2048,128]{1,0:T(8,128)(2,1)}, bf16[2048,128]{1,0:T(8,128)(2,1)}, bf16[1...) custom-call(bf16[128,512]{1,0:T(8,128)(2,1)S(1)} %get-tuple-element.24.refs_0_, ...), custom_call_target="tpu_custom_call" | custom-call | tf_op jit(solution)/shard_map/pallas_call | solution.py:700

commit v5 on v4

--- a/solution.py
+++ b/solution.py
@@ -563,12 +563,12 @@
     rtb[...] = jnp.where(lane2 == 0, mm(c0[...], backr[...]), mm(c1[...], backr[...])).astype(BF)
     home(rtb, srcr, zr_s, zr_r)
     srcr[seat(grp), :] = rtb[0:SEAT, :]
+    combine(2)
+    combine(3)
     landed(n_copies)
     norms = ((rnall[0] + rnall[1]) + rnall[2]) + rnall[3]
     gr_ref[...] = norms[0:16, :]
     ur_ref[...] = norms[16:32, :]
-    combine(2)
-    combine(3)
     landed(g_copies)
     total = jnp.zeros((128, 128), F32)
     for k in range(4):

time: 90.8 us -> 90.8 us (level)
  no operation moved by 1% of the time
where the time goes in v5:
time: 90.8 us; the launch traced here: 90.7 us
  Pallas kernels  90 us (99%)
    pallas_call x1, Pallas kernels, on_device(): pl.pallas_call(kernel, out_shape=outs, in_specs=[hbm] * 7, out_specs=(vme...  88.7 us

profile of v5, /device:TPU:1, one launch (start us, length us, event | category | flops | bytes accessed | tf_op | source)
XLA Modules:
  0.0 90.7 jit_solution(7319529985380852938)
XLA Ops:
  0.6 88.7 %shard_map.134 = (bf16[128,512]{1,0:T(8,128)(2,1)S(1)}, bf16[2,128]{1,0:T(2,128)(2,1)S(1)}, bf16[2048,128]{1,0:T(8,128)(2,1)S(1)}, bf16[2048,128]{1,0:T(8,128)(2...) custom-call(s32[2,128]{1,0:T(2,128)} %bitcast.14, ...), custom_call_target="tpu_custom_call" | custom-call | tf_op jit(solution)/shard_map/pallas_call | solution.py:692
  89.4 1.3 %shard_map.135 = (bf16[128,512]{1,0:T(8,128)(2,1)}, bf16[2,128]{1,0:T(2,128)(2,1)}, bf16[2048,128]{1,0:T(8,128)(2,1)}, bf16[2048,128]{1,0:T(8,128)(2,1)}, bf16[1...) custom-call(bf16[128,512]{1,0:T(8,128)(2,1)S(1)} %get-tuple-element.24.refs_0_, ...), custom_call_target="tpu_custom_call" | custom-call | tf_op jit(solution)/shard_map/pallas_call | solution.py:700
